TPU v7x, 32 devices: a whole 2x2x4 slice. The times are simulated.
32 devices in a mesh: sp: 16 (over z, y, core), tp: 2 (over x).
Axes of the slice: x: 2, y: 2, z: 4, core: 2. Of those that a mesh axis runs over, the one named last changes fastest.
Arguments:
- pool_input: bfloat16 [4, 128, 8192], P(None, 'tp', 'sp'), may hold values from -8 to 8
- doc_ids: int32 [8192], P('sp'), may hold values from 0 to 3, never falling along the last dimension, each value on 1 to 4096 neighbouring positions
- pool_map: bfloat16 [4, 128, 128], replicated, may hold values from -0.5 to 0.5
- pool_scale: float32 [512], replicated, may hold values from 0.1 to 1.9
- w_out: bfloat16 [512, 2048], replicated, may hold values from -0.25 to 0.25
- residual: bfloat16 [8192, 2048], P(('sp', 'tp')), may hold values from -6 to 6
- mix_gain: float32 [2048], replicated, may hold values from 0.1 to 1.9
- ffn_gain: float32 [2048], replicated, may hold values from 0.1 to 1.9
- out_gain: float32 [2048], replicated, may hold values from 0.1 to 1.9
- expert_ids: int32 [8192, 2], P(('sp', 'tp')), may hold values from 0 to 31, all different within a row; in each aligned block of 256 rows (0 to 255, 256 to 511, ...) at most 32 rows name the same one
- route_logits: float32 [8192, 2], P(('sp', 'tp')), may hold values from -6 to 6
- w_gate: bfloat16 [32, 2048, 1024], P(('sp', 'tp')), may hold values from -0.125 to 0.125
- w_up: bfloat16 [32, 2048, 1024], P(('sp', 'tp')), may hold values from -0.125 to 0.125
- w_down: bfloat16 [32, 1024, 2048], P(('sp', 'tp')), may hold values from -0.1875 to 0.1875
Outputs:
- layer_out: bfloat16 [8192, 2048], P(('sp', 'tp'))
Inputs may be any that keep to these rules, and one draw needn't show every extreme that they name: `doc_ids`: document numbers never fall along the positions; no document has more than 4096 positions. `expert_ids`: each row names 2 different experts; within each aligned block of 256 rows no expert is named by more than 32 rows, a bound that some block reaches.
All inputs are finite; a program needn't handle non-finite values.
Results may differ from a plain program's by a relative error of at most 0.03.
Values may be sent and summed in bfloat16 or wider, within the bound.
No kernel may reach another device: no remote copies, remote signals or barrier semaphores. Data moves between devices by JAX's collectives and lax.ppermute only.
A program may use at most 64 MiB of HBM per device.

v0:
```python
import jax
import jax.numpy as jnp
from jax import lax
from jax.sharding import PartitionSpec as P


def entering(value, axis, join, neutral):
    count, mine = (lax.axis_size(axis), lax.axis_index(axis))
    pieces = jax.tree.map(lambda part: lax.all_gather(part, axis), value)
    total = jax.tree.map(
        lambda part, zero: jnp.full_like(part, 0) + jnp.asarray(zero, part.dtype), value, neutral
    )

    def step(position, total):
        longer = join(total, jax.tree.map(lambda part: part[position], pieces))
        return jax.tree.map(lambda new, old: jnp.where(position < mine, new, old), longer, total)

    return lax.fori_loop(0, count - 1, step, total)


def passed_along(x, axis, by):
    devices = lax.axis_size(axis)
    pairs = [(i, i + by) for i in range(devices) if 0 <= i + by < devices]
    return lax.ppermute(x, axis, pairs)


def rms_scale(vector):
    return lax.rsqrt(jnp.mean(vector * vector, axis=-1, keepdims=True) + 1e-06)


def expert_rows(row_data, w_gate, w_up, w_down):
    gate_act = jnp.dot(row_data, w_gate[0], preferred_element_type=jnp.float32)
    up_act = jnp.dot(row_data, w_up[0], preferred_element_type=jnp.float32)
    hidden = (jax.nn.silu(gate_act) * up_act).astype(jnp.bfloat16)
    return jnp.dot(hidden, w_down[0], preferred_element_type=jnp.float32).astype(jnp.bfloat16)


def carry_combine(earlier, later):
    later_empty = later[2] < 0.0
    same_doc = earlier[2] == later[2]
    sums = jnp.where(later_empty, earlier[0], later[0] + jnp.where(same_doc, earlier[0], 0.0))
    counts = jnp.where(later_empty, earlier[1], later[1] + jnp.where(same_doc, earlier[1], 0.0))
    last_doc = jnp.where(later_empty, earlier[2], later[2])
    return (sums, counts, last_doc)


def local(
    pool_input,
    doc_ids,
    pool_map,
    pool_scale,
    w_out,
    residual,
    mix_gain,
    ffn_gain,
    out_gain,
    expert_ids,
    route_logits,
    w_gate,
    w_up,
    w_down,
):
    groups, channels, length = pool_input.shape
    values = pool_input.astype(jnp.float32)
    block_len = min(length, 128)
    block_count = length // block_len
    lower_tri = (jnp.arange(block_len)[:, None] <= jnp.arange(block_len)[None, :]).astype(
        jnp.float32
    )
    pieces = values.reshape(groups, channels, block_count, block_len)
    within = jnp.einsum("gcbk,kt->gcbt", pieces, lower_tri, precision=lax.Precision.HIGHEST)
    totals = within[..., -1]
    before_blocks = jnp.cumsum(totals, axis=2) - totals
    prefix = (within + before_blocks[..., None]).reshape(groups, channels, length)
    position = jnp.arange(length, dtype=jnp.int32)
    resets = jnp.concatenate([jnp.zeros((1,), bool), doc_ids[1:] != doc_ids[:-1]])
    starts = lax.cummax(jnp.where(resets, position, 0), axis=0)
    before = jnp.concatenate(
        [jnp.zeros((groups, channels, 1), jnp.float32), prefix[:, :, :-1]], axis=2
    )
    local_run = prefix - jnp.take(before, starts, axis=2)
    local_count = (position - starts + 1).astype(jnp.float32)
    last_id = doc_ids[-1].astype(jnp.float32)
    identity = (
        jnp.zeros((groups, channels), jnp.float32),
        jnp.zeros((), jnp.float32),
        jnp.full((), -1.0, jnp.float32),
    )
    carried = entering(
        (local_run[:, :, -1], local_count[-1], last_id), "sp", carry_combine, identity
    )
    joined = doc_ids.astype(jnp.float32) == carried[2]
    running = local_run + jnp.where(joined, carried[0][..., None], 0.0)
    doc_position = local_count + jnp.where(joined, carried[1], 0.0)
    diff_list = []
    for group_idx in range(groups):
        span_len = length * 2**group_idx
        far_rows = passed_along(
            running[group_idx].astype(jnp.bfloat16), "sp", 2**group_idx
        ).astype(jnp.float32)
        window = running[group_idx] - jnp.where(doc_position > span_len, far_rows, 0.0)
        window_mean = window / jnp.minimum(doc_position, float(span_len))
        diff_list.append((window_mean - values[group_idx]).astype(jnp.bfloat16))
    pool_diff = jnp.stack(diff_list)
    by_token = lax.all_to_all(pool_diff, "tp", split_axis=2, concat_axis=1, tiled=True)
    row_count = by_token.shape[2]
    mapped = jnp.einsum(
        "gct,gcd->tgd", by_token, pool_map, preferred_element_type=jnp.float32
    ).reshape(row_count, -1)
    mapped = (mapped * pool_scale).astype(jnp.bfloat16)
    projected = jnp.dot(mapped, w_out, preferred_element_type=jnp.float32)
    stream = (residual.astype(jnp.float32) + mix_gain * projected * rms_scale(projected)).astype(
        jnp.bfloat16
    )
    stream_back = stream.astype(jnp.float32)
    normed = (ffn_gain * stream_back * rms_scale(stream_back)).astype(jnp.bfloat16)
    top_count = expert_ids.shape[1]
    width = normed.shape[1]
    experts = w_gate.shape[0] * lax.axis_size("sp") * lax.axis_size("tp")
    capacity = max(2, 2 * row_count * top_count // experts)
    flat_expert = expert_ids.reshape(-1)
    onehot = (flat_expert[:, None] == jnp.arange(experts, dtype=jnp.int32)[None, :]).astype(
        jnp.int32
    )
    slot_rank = jnp.sum((jnp.cumsum(onehot, axis=0) - onehot) * onehot, axis=1)
    slot_index = flat_expert * capacity + slot_rank
    source_row = jnp.arange(row_count * top_count, dtype=jnp.int32) // top_count
    slot_row = jnp.full((experts * capacity,), row_count, jnp.int32).at[slot_index].set(source_row)
    padded = jnp.concatenate([normed, jnp.zeros((1, width), jnp.bfloat16)], axis=0)
    outgoing = padded[slot_row].reshape(experts, capacity, width)
    arrived = lax.all_to_all(outgoing, ("sp", "tp"), split_axis=0, concat_axis=0, tiled=True)
    finished = expert_rows(arrived.reshape(-1, width), w_gate, w_up, w_down).reshape(arrived.shape)
    results = lax.all_to_all(
        finished, ("sp", "tp"), split_axis=0, concat_axis=0, tiled=True
    ).reshape(-1, width)
    gathered = results[slot_index].astype(jnp.float32).reshape(row_count, top_count, width)
    weights = jax.nn.sigmoid(route_logits - route_logits[:, ::-1])
    expert_sum = jnp.sum(weights[..., None] * gathered, axis=1)
    return (stream_back + out_gain * expert_sum * rms_scale(expert_sum)).astype(jnp.bfloat16)


def solution(mesh):
    in_specs = (
        P(None, "tp", "sp"),
        P("sp"),
        P(),
        P(),
        P(),
        P(("sp", "tp"), None),
        P(),
        P(),
        P(),
        P(("sp", "tp"), None),
        P(("sp", "tp"), None),
        P(("sp", "tp"), None, None),
        P(("sp", "tp"), None, None),
        P(("sp", "tp"), None, None),
    )
    out_specs = P(("sp", "tp"), None)
    return jax.shard_map(local, mesh=mesh, in_specs=in_specs, out_specs=out_specs, check_vma=False)
```

profile of v0, /device:TPU:0, one launch (start us, length us, event | category | flops | bytes accessed | tf_op | source)
XLA Modules:
  0.0 397.7 jit_solution(14159232634341501602)
XLA Ops:
  0.0 1.3 convolution_bitcast_fusion
  2.1 1.3 copy.66
  3.4 0.8 slice_compare_fusion
  5.0 2.4 concatenate.13
  7.4 3.7 gather_fusion
  11.1 2.3 copy.54
  13.4 1.2 bitcast_subtract_fusion
  14.8 23.2 %all-gather = f32[64,64,1]{1,2,0:T(1,128)S(1)} all-gather(f32[4,64,1]{1,2,0:T(1,128)S(1)} %copy.55), channel_id=2, replica_groups=mesh['sp'=16,'tp'=2] {'sp'}, dimensions={0}, use_global_device_ids=true | all-gather | bytes 17408 | tf_op jit(solution)/shard_map/all_gather | solution.py:9
  38.6 0.7 convert_dynamic-update-slice_fusion
  39.3 0.7 slice_dynamic-update-slice_fusion
  40.1 29.8 %all-reduce.4 = (f32[16]{0:T(128)S(1)}, f32[16]{0:T(128)S(1)}) all-reduce(f32[16]{0:T(128)S(1)} %convert_dynamic-update-slice_fusion, f32[16]{0:T(128)S(1)} %slice_dynamic-update-slice_fusion), channel_id=1, replica_groups=mesh['sp'=16,'tp'=2] {'sp'}, use_global_device_ids=true, to_apply=%add.2 | all-reduce | flops 32 | bytes 256
  69.9 54.2 %while.18 = (s32[]{:T(128)}, f32[4,64]{1,0:T(4,128)S(1)}, f32[]{:T(128)}, f32[]{:T(128)}, s32[]{:T(128)}, /*index=5*/f32[16]{0:T(128)S(1)}, f32[16,4,64]{2,1,0:T...) while((s32[]{:T(128)}, f32[4,64]{1,0:T(4,128)S(1)}, f32[]{:T(128)}, ...), condition=%wide.region_4.5_spmd.clone, body=%wide.region_3.4_spmd.clone.sunk | while | flops 1292 | bytes 3326 | solution.py:18
  71.0 0.7 dynamic_slice.30
  74.6 0.7 dynamic_slice.30
  77.1 0.6 dynamic_slice.29
  78.3 0.7 dynamic_slice.30
  80.7 0.6 dynamic_slice.29
  81.9 0.7 dynamic_slice.30
  84.3 0.6 dynamic_slice.29
  85.5 0.7 dynamic_slice.30
  89.1 0.7 dynamic_slice.30
  92.7 0.7 dynamic_slice.30
  95.2 0.6 dynamic_slice.29
  96.3 0.7 dynamic_slice.30
  98.8 0.6 dynamic_slice.29
  99.9 0.7 dynamic_slice.30
  102.4 0.6 dynamic_slice.29
  103.5 0.7 dynamic_slice.30
  107.2 0.7 dynamic_slice.30
  110.8 0.7 dynamic_slice.30
  113.2 0.6 dynamic_slice.29
  114.4 0.7 dynamic_slice.30
  118.0 0.7 dynamic_slice.30
  121.6 0.7 dynamic_slice.30
  124.1 0.6 broadcast_compare_fusion.3
  124.8 0.7 fusion.27
  125.5 1.9 collective-permute-start.1
  127.4 2.0 collective-permute-start
  129.4 1.9 collective-permute-start.2
  131.3 3.1 collective-permute-start.3
  134.5 0.6 broadcast_compare_fusion.2
  135.1 0.8 copy.61
  136.2 0.7 broadcast_multiply_fusion
  136.9 1.2 reduce-window.19
  138.8 2.4 scatter_custom_fusion
  141.3 0.9 fusion.38
  142.2 1.0 fusion.37
  143.6 1.1 reshape.220
  144.7 3.6 all-to-all-start
  148.3 5.1 %all-to-all-done = bf16[2,2,32768]{2,1,0:T(2,128)(2,1)S(1)} async-done(((bf16[2,2,32768]{2,1,0:T(2,128)(2,1)}), bf16[2,2,32768]{2,1,0:T(2,128)(2,1)S(1)}, u32[]{:S(2)}, u32[]{:S(2)}) %all-to-all-start) | async-done | bytes 262176 | tf_op jit(solution)/shard_map/all_to_all | solution.py:105
  154.5 0.8 multiply_reduce_fusion.2
  155.4 0.6 fusion.13
  156.0 1.0 copy-done.1
  157.3 6.0 %gather_fusion.1 = bf16[1024,2048]{1,0:T(8,128)(2,1)} fusion(bf16[257,2048]{1,0:T(8,128)(2,1)S(1)} %concatenate.14, s32[1024]{0:T(1024)S(1)} %fusion.41), kind=kCustom, calls=%fused_computation.1 | custom fusion | bytes 8392704 | tf_op jit(solution)/shard_map/gather | solution.py:130
  163.4 96.9 %all_to_all.28 = bf16[32,32,2048]{2,1,0:T(8,128)(2,1)S(1)} all-to-all(bf16[32,32,2048]{2,1,0:T(8,128)(2,1)} %bitcast.186), channel_id=1, replica_groups=mesh['sp'=16,'tp'=2] {'sp','tp'}, dimensions={0} | all-to-all | bytes 8388608 | tf_op jit(solution)/shard_map/all_to_all | solution.py:131
  260.3 4.5 %fusion.2 = f32[1024,1024]{1,0:T(8,128)S(1)} fusion(bf16[1024,2048]{1,0:T(8,128)(2,1)S(1)} %bitcast.188, bf16[1,2048,1024]{2,1,0:T(8,128)(2,1)S(1)} %copy-done.12), kind=kOutput, calls=%fused_computation.8 | convolution fusion | flops 4294967296 | bytes 12582912 | tf_op jit(solution)/shard_map/dot_general | solution.py:33
  264.8 5.4 %multiply_convert_fusion = bf16[1024,1024]{1,0:T(8,128)(2,1)S(1)} fusion(f32[1024,1024]{1,0:T(8,128)S(1)} %fusion.2, bf16[1024,2048]{1,0:T(8,128)(2,1)S(1)} %bitcast.189, bf16[1,2048,1024]{2,1,0:T(8,128)(2,1)S(1)} %copy-done.13), kind=kOutput, calls=%fused_computation.13 | convolution fusion | flops 4301258752 | bytes 14680064 | tf_op jit(solution)/shard_map/dot_general | solution.py:32
  270.2 6.1 %fusion.6 = bf16[1024,2048]{1,0:T(8,128)(2,1)} fusion(bf16[1024,1024]{1,0:T(8,128)(2,1)S(1)} %multiply_convert_fusion, bf16[1,1024,2048]{2,1,0:T(8,128)(2,1)S(1)} %copy-done.14), kind=kOutput, calls=%fused_computation.14 | convolution fusion | flops 4297064448 | bytes 10485760 | tf_op jit(solution)/shard_map/dot_general | solution.py:35
  276.3 3.9 all-to-all-start.2
  280.5 93.2 %all-to-all-done.2 = bf16[32,32,2048]{2,1,0:T(8,128)(2,1)} async-done(((bf16[32,32,2048]{2,1,0:T(8,128)(2,1)}), bf16[32,32,2048]{2,1,0:T(8,128)(2,1)}, u32[]{:S(2)}, u32[]{:S(2)}) %all-to-all-start.2) | async-done | bytes 4194336 | tf_op jit(solution)/shard_map/all_to_all | solution.py:133
  373.7 8.0 %gather_fusion.2 = bf16[512,2048]{1,0:T(8,128)(2,1)} fusion(bf16[1024,2048]{1,0:T(8,128)(2,1)} %bitcast.36, s32[1024]{0:T(1024)S(1)} %pad_clamp_fusion), kind=kCustom, calls=%fused_computation.2 | custom fusion | bytes 4196352 | tf_op jit(solution)/shard_map/gather | solution.py:136
  381.7 5.4 %reshape.169 = f32[256,2,2048]{2,1,0:T(2,128)} reshape(bf16[512,2048]{1,0:T(8,128)(2,1)} %gather_fusion.2) | data formatting | bytes 6291456 | tf_op jit(solution)/shard_map/convert_element_type | solution.py:136
  387.1 9.0 %multiply_reduce_fusion = f32[256,2048]{1,0:T(8,128)S(1)} fusion(f32[256,2,2048]{2,1,0:T(2,128)} %reshape.169, f32[256,2]{1,0:T(8,128)S(1)} %copy.59), kind=kLoop, calls=%fused_computation.12 | loop fusion | flops 1572864 | bytes 6293504 | tf_op jit(solution)/shard_map/reduce_sum | solution.py:138
  396.4 1.3 fusion.14
  (106 shorter events, 10.5 us)
Async XLA Ops:
  0.0 154.5 %copy-start = (bf16[512,2048]{1,0:T(8,128)(2,1)S(1)}, bf16[512,2048]{1,0:T(8,128)(2,1)}, u32[]{:S(2)}) copy-start(bf16[512,2048]{1,0:T(8,128)(2,1)} %param.20) | copy-start | bytes 6291460
  2.1 36.0 %copy-start.15 = (u32[32]{0:T(128)S(1)}, u32[32]{0:T(128)}, u32[]{:S(2)}) copy-start(u32[32]{0:T(128)} %constant.127) | copy-start | bytes 388
  2.1 36.6 %copy-start.6 = (s32[512]{0:T(512)S(1)}, s32[512]{0:T(512)}, u32[]{:S(2)}) copy-start(s32[512]{0:T(512)} %param.17) | copy-start | bytes 6148
  5.0 130.1 %copy-start.3 = (bf16[4,64,512]{2,1,0:T(8,128)(2,1)S(1)}, bf16[4,64,512]{2,1,0:T(8,128)(2,1)}, u32[]{:S(2)}) copy-start(bf16[4,64,512]{2,1,0:T(8,128)(2,1)} %param.16) | copy-start | bytes 786436
  124.8 29.3 %copy-start.5 = (bf16[4,128,128]{2,1,0:T(8,128)(2,1)S(1)}, bf16[4,128,128]{2,1,0:T(8,128)(2,1)}, u32[]{:S(2)}) copy-start(bf16[4,128,128]{2,1,0:T(8,128)(2,1)} %param.18) | copy-start | bytes 393220
  125.5 15.8 %collective-permute-start.1 = (bf16[64,512]{1,0:T(8,128)(2,1)}, bf16[64,512]{1,0:T(8,128)(2,1)}, u32[]{:S(2)}, u32[]{:S(2)}) collective-permute-start(bf16[64,512]{1,0:T(8,128)(2,1)} %get-tuple-element.207), channel_id=1, source_target_pairs={{0,4},{2,6},{4,8},{6,10},{8,12},{10,14},{12,16},{14,18},{16,20},{1... | collective-permute-start | bytes 196616 | tf_op jit(solution)/shard_map/ppermute | solution.py:24
  127.4 14.8 %collective-permute-start = (bf16[64,512]{1,0:T(8,128)(2,1)}, bf16[64,512]{1,0:T(8,128)(2,1)}, u32[]{:S(2)}, u32[]{:S(2)}) collective-permute-start(bf16[64,512]{1,0:T(8,128)(2,1)} %get-tuple-element.204), channel_id=1, source_target_pairs={{0,2},{2,4},{4,6},{6,8},{8,10},{10,12},{12,14},{14,16},{16,18},{18... | collective-permute-start | bytes 196616 | tf_op jit(solution)/shard_map/ppermute | solution.py:24
  129.4 12.7 %collective-permute-start.2 = (bf16[64,512]{1,0:T(8,128)(2,1)}, bf16[64,512]{1,0:T(8,128)(2,1)}, u32[]{:S(2)}, u32[]{:S(2)}) collective-permute-start(bf16[64,512]{1,0:T(8,128)(2,1)} %get-tuple-element.206), channel_id=1, source_target_pairs={{0,8},{2,10},{4,12},{6,14},{8,16},{10,18},{12,20},{14,22},{16,24},... | collective-permute-start | bytes 196616 | tf_op jit(solution)/shard_map/ppermute | solution.py:24
  131.3 10.8 %collective-permute-start.3 = (bf16[64,512]{1,0:T(8,128)(2,1)}, bf16[64,512]{1,0:T(8,128)(2,1)}, u32[]{:S(2)}, u32[]{:S(2)}) collective-permute-start(bf16[64,512]{1,0:T(8,128)(2,1)} %get-tuple-element.205), channel_id=1, source_target_pairs={{0,16},{2,18},{4,20},{6,22},{8,24},{10,26},{12,28},{14,30},{1,17},... | collective-permute-start | bytes 196616 | tf_op jit(solution)/shard_map/ppermute | solution.py:24
  135.1 19.3 %copy-start.11 = (f32[512]{0:T(512)S(1)}, f32[512]{0:T(512)}, u32[]{:S(2)}) copy-start(f32[512]{0:T(512)} %param.19) | copy-start | bytes 6148
  144.7 10.7 %copy-start.7 = (f32[2048]{0:T(1024)S(1)}, f32[2048]{0:T(1024)}, u32[]{:S(2)}) copy-start(f32[2048]{0:T(1024)} %param.22) | copy-start | bytes 24580
  144.7 8.7 %all-to-all-start = ((bf16[2,2,32768]{2,1,0:T(2,128)(2,1)}), bf16[2,2,32768]{2,1,0:T(2,128)(2,1)S(1)}, u32[]{:S(2)}, u32[]{:S(2)}) async-start(bf16[2,2,32768]{2,1,0:T(2,128)(2,1)} %reshape.220), calls=%async_computation | async-start | bytes 524288 | tf_op jit(solution)/shard_map/all_to_all | solution.py:105
  154.1 1.3 copy-start.4
  154.5 2.4 copy-start.8
  156.0 1.0 copy-start.1
  163.4 96.9 %copy-start.12 = (bf16[1,2048,1024]{2,1,0:T(8,128)(2,1)S(1)}, bf16[1,2048,1024]{2,1,0:T(8,128)(2,1)}, u32[]{:S(2)}) copy-start(bf16[1,2048,1024]{2,1,0:T(8,128)(2,1)} %param.28) | copy-start | bytes 12582916
  260.3 4.5 %copy-start.13 = (bf16[1,2048,1024]{2,1,0:T(8,128)(2,1)S(1)}, bf16[1,2048,1024]{2,1,0:T(8,128)(2,1)}, u32[]{:S(2)}) copy-start(bf16[1,2048,1024]{2,1,0:T(8,128)(2,1)} %param.27) | copy-start | bytes 12582916
  264.8 5.4 %copy-start.14 = (bf16[1,1024,2048]{2,1,0:T(8,128)(2,1)S(1)}, bf16[1,1024,2048]{2,1,0:T(8,128)(2,1)}, u32[]{:S(2)}) copy-start(bf16[1,1024,2048]{2,1,0:T(8,128)(2,1)} %param.29) | copy-start | bytes 12582916
  276.3 3.9 copy-start.10
  276.3 97.4 %all-to-all-start.2 = ((bf16[32,32,2048]{2,1,0:T(8,128)(2,1)}), bf16[32,32,2048]{2,1,0:T(8,128)(2,1)}, u32[]{:S(2)}, u32[]{:S(2)}) async-start(bf16[32,32,2048]{2,1,0:T(8,128)(2,1)} %bitcast.187), calls=%async_computation.2 | async-start | bytes 8388608 | tf_op jit(solution)/shard_map/all_to_all | solution.py:133
  387.1 9.2 %copy-start.2 = (bf16[256,2048]{1,0:T(8,128)(2,1)S(1)}, bf16[256,2048]{1,0:T(8,128)(2,1)}, u32[]{:S(2)}) copy-start(bf16[256,2048]{1,0:T(8,128)(2,1)} %copy-done.1) | copy-start | bytes 3145732
  387.1 9.2 %copy-start.9 = (f32[2048]{0:T(1024)S(1)}, f32[2048]{0:T(1024)}, u32[]{:S(2)}) copy-start(f32[2048]{0:T(1024)} %param.24) | copy-start | bytes 24580
where the time goes:
time: 399 us; the launch traced here: 398 us
  blocking collectives  150 us (38%)
  waiting for transfers between devices  98.3 us (25%)
  local copies, waits for them, and re-layouts  57.5 us (14%)
  loops' own time  35.5 us (9%)
  other arithmetic  21.1 us (5%)
  matrix products  18.4 us (5%)
  starting transfers between devices  16.5 us (4%)
    all_to_all x1, blocking collectives, local(): lax.all_to_all(outgoing, ('sp', 'tp'), split_axis=0, concat_axis=0, tiled...  96.9 us
    all_to_all x1, waiting for transfers between devices, local(): lax.all_to_all(finished, ('sp', 'tp'), split_axis=0, concat_axis=0, tiled...  93.2 us
    another operation x1, loops' own time, entering(): return lax.fori_loop(0, count - 1, step, total)  35.5 us
    unnamed x1, blocking collectives  29.8 us
    all_gather x1, blocking collectives, entering(): pieces = jax.tree.map(lambda part: lax.all_gather(part, axis), value)  23.2 us
    dynamic_slice x30, local copies, waits for them, and re-layouts, step(): longer = join(total, jax.tree.map(lambda part: part[position], pieces))  18.5 us
    ppermute x4, starting transfers between devices, passed_along(): return lax.ppermute(x, axis, pairs)  8.98 us
    reduce_sum x1, other arithmetic, local(): expert_sum = jnp.sum(weights[..., None] * gathered, axis=1)  8.96 us
  transfers between devices with their start and end apart: 6, of which 2 were waited for; matrix products, arithmetic and copies ran while one was open for 2% of the time, Pallas kernels for 0%

commit v1 on v0

v1 whole, which is shorter than its diff:
```python
import jax
import jax.numpy as jnp
from jax import lax
from jax.sharding import Mesh, PartitionSpec as P

BF16, F32 = jnp.bfloat16, jnp.float32
SP = ("zh", "sl")
HALF = ("sl", "tp")
ALL = ("zh", "sl", "tp")


def to_twin(x):
    return lax.ppermute(x, "zh", [(0, 1), (1, 0)])


def passed_along(x, by):
    devices = lax.axis_size("zh") * lax.axis_size("sl")
    return lax.ppermute(x, SP, [(i, i + by) for i in range(devices - by)])


def rms_scale(vector):
    return lax.rsqrt(jnp.mean(vector * vector, axis=-1, keepdims=True) + 1e-06)


def dot(a, b):
    return jnp.dot(a, b, preferred_element_type=F32)


def dot_t(a, b):
    return lax.dot_general(a, b, (((0,), (0,)), ((), ())), preferred_element_type=F32)


def expert_rows(rows, w_gate, w_up, w_down):
    hidden = (jax.nn.silu(dot(rows, w_gate[0])) * dot(rows, w_up[0])).astype(BF16)
    return dot(hidden, w_down[0]).astype(BF16)


def mixed(mapped, residual, w_out, mix_gain, ffn_gain):
    projected = dot(mapped, w_out)
    stream = residual.astype(F32) + mix_gain * projected * rms_scale(projected)
    stream = lax.reduce_precision(stream, 8, 7)
    return stream, (ffn_gain * stream * rms_scale(stream)).astype(BF16)


def routes(ids, logits, first, experts, capacity):
    rows = ids.shape[1]
    expert = jnp.arange(experts, dtype=F32)[:, None]
    named = [(ids[k : k + 1] - first == expert) for k in range(2)]
    held = (named[0] | named[1]).astype(BF16)
    at = jnp.arange(rows)
    earlier = (at[:, None] < at[None, :]).astype(BF16)
    rank = dot(held, earlier)
    slots = [
        jnp.sum(jnp.where(n, expert * capacity + rank + 1.0, 0.0), axis=0, keepdims=True) - 1.0
        for n in named
    ]
    slot = jnp.arange(experts * capacity, dtype=F32)[:, None]
    hits = [slot == s for s in slots]
    pick = (hits[0] | hits[1]).astype(BF16)
    weights = [
        jax.nn.sigmoid(logits[0:1] - logits[1:2]),
        jax.nn.sigmoid(logits[1:2] - logits[0:1]),
    ]
    weight = jnp.where(hits[0], weights[0], 0.0) + jnp.where(hits[1], weights[1], 0.0)
    high = lax.reduce_precision(weight, 8, 7)
    return pick, high.astype(BF16), (weight - high).astype(BF16)


def local(
    pool_input,
    doc_ids,
    pool_map,
    pool_scale,
    w_out,
    residual,
    mix_gain,
    ffn_gain,
    out_gain,
    expert_ids,
    route_logits,
    w_gate,
    w_up,
    w_down,
):
    groups, channels, length = pool_input.shape
    tp = lax.axis_size("tp")
    blocks = lax.axis_size("zh") * lax.axis_size("sl")
    mine = lax.axis_index(SP)
    rows, width = residual.shape
    experts = w_gate.shape[0] * lax.axis_size("sl") * tp
    capacity = max(2, rows * expert_ids.shape[1] // experts)

    far_blocks = [passed_along(pool_input[g], 2**g) for g in range(groups)]
    far_residual = to_twin(residual)

    flat = pool_input.reshape(groups * channels, length)
    at = jnp.arange(length, dtype=jnp.int32)
    same = doc_ids[:, None] == doc_ids[None, :]
    within = ((at[:, None] <= at[None, :]) & same).astype(BF16)
    tail = (doc_ids == doc_ids[-1])[None, :]
    tail_sums = lax.dot_general(
        tail.astype(BF16), flat, (((1,), (1,)), ((), ())), preferred_element_type=F32
    ).reshape(-1)
    tail_count = jnp.sum(tail.astype(F32))
    meta = jnp.stack([tail_count, doc_ids[-1].astype(F32)])
    ids_t = expert_ids.astype(F32).T
    logits_t = route_logits.T
    parts = [tail_sums, jnp.pad(meta, (0, 126)), ids_t.reshape(-1), logits_t.reshape(-1)]
    sizes = [p.shape[0] for p in parts]
    payload = jnp.concatenate(parts)
    payload = jnp.pad(payload, (0, -payload.shape[0] % 1024)).reshape(-1, 128)
    news = lax.all_to_all(
        jnp.broadcast_to(payload[None], (blocks,) + payload.shape), SP, 0, 0, tiled=True
    )
    news = news.reshape(blocks, -1)
    sums = news[:, : sizes[0]]
    counts = news[:, sizes[0]][:, None]
    lasts = news[:, sizes[0] + 1][:, None]
    block = jnp.arange(blocks, dtype=jnp.int32)[:, None]
    joins = (block < mine) & (lasts == doc_ids[0].astype(F32))
    reach = 2 ** (jnp.arange(groups * channels, dtype=jnp.int32) // channels)[None, :]
    between_on = (block < mine) & (block > mine - reach)
    carry = jnp.sum(jnp.where(joins, sums, 0.0), axis=0)[:, None]
    between = jnp.sum(jnp.where(between_on, sums, 0.0), axis=0)[:, None]
    carry_count = jnp.sum(jnp.where(joins, counts, 0.0))

    local_run = dot(flat, within)
    first_doc = (doc_ids == doc_ids[0])[None, :]
    local_count = jnp.sum(within.astype(F32), axis=0, keepdims=True)
    position = local_count + jnp.where(first_doc, carry_count, 0.0)
    after = (at[:, None] > at[None, :]).astype(BF16)
    far_sum = dot(jnp.concatenate(far_blocks, axis=0), after)
    span = (length * reach.reshape(-1, 1)).astype(F32)
    started = position > span
    window = local_run + jnp.where(
        started, between + far_sum, jnp.where(first_doc, carry, 0.0)
    )
    diff = (window / jnp.minimum(position, span) - flat.astype(F32)).astype(BF16)

    diff = diff.reshape(groups, channels, tp, rows).transpose(2, 0, 1, 3)
    by_row = lax.all_to_all(diff, "tp", 0, 0, tiled=True)
    maps = pool_map.reshape(groups, tp, channels, -1)
    mapped = jnp.concatenate(
        [
            dot_t(by_row[:, g].reshape(tp * channels, rows), maps[g].reshape(tp * channels, -1))
            for g in range(groups)
        ],
        axis=1,
    )
    mapped = (mapped * pool_scale).astype(BF16)
    far_mapped = to_twin(mapped)

    half = lax.axis_index("zh")
    twin = (1 - half) * (blocks // 2) + lax.axis_index("sl")
    first = (half * experts).astype(F32)
    base = sizes[0] + sizes[1]
    twin_news = lax.dynamic_index_in_dim(news, twin, 0, keepdims=False)
    twin_ids = twin_news[base : base + 2 * rows].reshape(2, rows)
    twin_logits = twin_news[base + 2 * rows : base + 4 * rows].reshape(2, rows)
    own_pick, own_high, own_low = routes(ids_t, logits_t, first, experts, capacity)
    far_pick, far_high, far_low = routes(twin_ids, twin_logits, first, experts, capacity)

    def there(send):
        send = send.reshape(experts, capacity, width)
        return lax.all_to_all(send, HALF, 0, 0, tiled=True).reshape(-1, width)

    stream, normed = mixed(mapped, residual, w_out, mix_gain, ffn_gain)
    own_in = there(dot(own_pick, normed).astype(BF16))
    _, far_normed = mixed(far_mapped, far_residual, w_out, mix_gain, ffn_gain)
    far_in = there(dot(far_pick, far_normed).astype(BF16))
    own_out = expert_rows(own_in, w_gate, w_up, w_down)
    far_out = expert_rows(far_in, w_gate, w_up, w_down)
    far_back = there(far_out)
    far_part = (dot_t(far_high, far_back) + dot_t(far_low, far_back)).astype(BF16)
    other_part = to_twin(far_part)
    own_back = there(own_out)
    expert_sum = dot_t(own_high, own_back) + dot_t(own_low, own_back) + other_part.astype(F32)
    return (stream + out_gain * expert_sum * rms_scale(expert_sum)).astype(BF16)


def solution(mesh):
    sp, tp = mesh.shape["sp"], mesh.shape["tp"]
    fine = Mesh(mesh.devices.reshape(2, sp // 2, tp), ALL)
    rowwise = P(ALL, None)
    each = P(ALL, None, None)
    in_specs = (
        P(None, "tp", SP),
        P(SP),
        P(),
        P(),
        P(),
        rowwise,
        P(),
        P(),
        P(),
        rowwise,
        rowwise,
        each,
        each,
        each,
    )
    return jax.shard_map(local, mesh=fine, in_specs=in_specs, out_specs=rowwise, check_vma=False)
```

time: 399 us -> 258 us (0.65)
  blocking collectives: 150 us -> 0 us
  local copies, waits for them, and re-layouts: 57.5 us -> 5.95 us
  starting transfers between devices: 16.5 us -> 66.2 us
  matrix products: 18.4 us -> 60.2 us
  loops' own time: 35.5 us -> 0 us
  waiting for transfers between devices: 98.3 us -> 112 us
  other arithmetic: 21.1 us -> 10.9 us
    all_to_all x1 -> x0, blocking collectives: 96.9 us -> none  [local(): lax.all_to_all(outgoing, ('sp', 'tp'), split_axis=0, concat_axis=0, tiled...]
    dot_general x6 -> x21, matrix products: 18.4 us -> 60.2 us  [the longest x12 47.5 us: dot(): return jnp.dot(a, b, preferred_element_type=F32)]
    another operation x1 -> x0, loops' own time: 35.5 us -> none  [entering(): return lax.fori_loop(0, count - 1, step, total)]
    ppermute x4 -> x7, starting transfers between devices: 8.98 us -> 40.4 us  [the longest x3 26.2 us: to_twin(): return lax.ppermute(x, 'zh', [(0, 1), (1, 0)])]
    unnamed x1 -> x0, blocking collectives: 29.8 us -> none
    ppermute x4 -> x7, waiting for transfers between devices: 0.01 us -> 24.1 us  [the longest x3 24.1 us: to_twin(): return lax.ppermute(x, 'zh', [(0, 1), (1, 0)])]
    all_gather x1 -> x0, blocking collectives: 23.2 us -> none  [entering(): pieces = jax.tree.map(lambda part: lax.all_gather(part, axis), value)]
    gather x4 -> x0, local copies, waits for them, and re-layouts: 20 us -> none  [the longest x1 8 us: local(): results[slot_index].astype(jnp.float32).reshape(row_count, top_count, width)]
  transfers between devices with their start and end apart: 6 -> 13, of which waited for: 2 -> 8; matrix products, arithmetic and copies ran while one was open for 2% -> 25% of each run, Pallas kernels for 0% -> 0%
where the time goes in v1:
time: 258 us; the launch traced here: 257 us
  waiting for transfers between devices  112 us (43%)
  starting transfers between devices  66.2 us (26%)
  matrix products  60.2 us (23%)
  other arithmetic  10.9 us (4%)
  local copies, waits for them, and re-layouts  5.95 us (2%)
    all_to_all x4, waiting for transfers between devices, there(): return lax.all_to_all(send, HALF, 0, 0, tiled=True).reshape(-1, width)  82.6 us
    dot_general x12, matrix products, dot(): return jnp.dot(a, b, preferred_element_type=F32)  47.5 us
    ppermute x3, starting transfers between devices, to_twin(): return lax.ppermute(x, 'zh', [(0, 1), (1, 0)])  26.2 us
    ppermute x3, waiting for transfers between devices, to_twin(): return lax.ppermute(x, 'zh', [(0, 1), (1, 0)])  24.1 us
    all_to_all x4, starting transfers between devices, there(): return lax.all_to_all(send, HALF, 0, 0, tiled=True).reshape(-1, width)  18.9 us
    ppermute x4, starting transfers between devices, passed_along(): return lax.ppermute(x, SP, [(i, i + by) for i in range(devices - by)])  14.2 us
    dot_general x8, matrix products, dot_t(): lax.dot_general(a, b, (((0,), (0,)), ((), ())), preferred_element_type=F32)  11.6 us
  transfers between devices with their start and end apart: 13, of which 8 were waited for; matrix products, arithmetic and copies ran while one was open for 25% of the time, Pallas kernels for 0%

profile of v1, /device:TPU:0, one launch (start us, length us, event | category | flops | bytes accessed | tf_op | source)
XLA Modules:
  0.0 257.3 jit_solution(12221397742061282049)
XLA Ops:
  0.0 1.1 slice_bitcast_fusion.3
  1.1 6.0 %collective-permute-start.3 = (bf16[64,512]{1,0:T(8,128)(2,1)S(1)}, bf16[64,512]{1,0:T(8,128)(2,1)S(1)}, u32[]{:S(2)}, u32[]{:S(2)}) collective-permute-start(bf16[64,512]{1,0:T(8,128)(2,1)S(1)} %get-tuple-element.25), channel_id=1, source_target_pairs={{0,16},{2,18},{4,20},{6,22},{8,24},{10,26},{12,28},{14,30},{1,17},... | collective-permute-start | bytes 196616 | tf_op jit(solution)/shard_map/ppermute | solution.py:18
  7.1 3.5 %collective-permute-start.2 = (bf16[64,512]{1,0:T(8,128)(2,1)S(1)}, bf16[64,512]{1,0:T(8,128)(2,1)S(1)}, u32[]{:S(2)}, u32[]{:S(2)}) collective-permute-start(bf16[64,512]{1,0:T(8,128)(2,1)S(1)} %get-tuple-element.26), channel_id=1, source_target_pairs={{0,8},{2,10},{4,12},{6,14},{8,16},{10,18},{12,20},{14,22},{16,24},... | collective-permute-start | bytes 196616 | tf_op jit(solution)/shard_map/ppermute | solution.py:18
  10.6 3.4 %collective-permute-start.1 = (bf16[64,512]{1,0:T(8,128)(2,1)S(1)}, bf16[64,512]{1,0:T(8,128)(2,1)S(1)}, u32[]{:S(2)}, u32[]{:S(2)}) collective-permute-start(bf16[64,512]{1,0:T(8,128)(2,1)S(1)} %get-tuple-element.24), channel_id=1, source_target_pairs={{0,4},{2,6},{4,8},{6,10},{8,12},{10,14},{12,16},{14,18},{16,20},{1... | collective-permute-start | bytes 196616 | tf_op jit(solution)/shard_map/ppermute | solution.py:18
  14.0 1.3 collective-permute-start
  15.3 1.3 fusion.121
  17.3 1.9 convert_reduce_fusion.1
  19.3 0.7 copy.46
  19.9 0.7 convert_bitcast_fusion.1
  20.6 0.7 fusion.111
  21.3 1.1 fusion.122
  22.5 0.7 broadcast_in_dim.138
  23.1 3.5 %all-to-all-start = ((f32[16,16,128]{2,1,0:T(8,128)}), f32[16,16,128]{2,1,0:T(8,128)S(1)}, u32[]{:S(2)}, u32[]{:S(2)}) async-start(f32[16,16,128]{2,1,0:T(8,128)} %broadcast_in_dim.138), calls=%async_computation | async-start | bytes 262144 | tf_op jit(solution)/shard_map/all_to_all | solution.py:112
  26.7 2.8 %collective-permute-start.4 = (bf16[256,2048]{1,0:T(8,128)(2,1)}, bf16[256,2048]{1,0:T(8,128)(2,1)}, u32[]{:S(2)}, u32[]{:S(2)}) collective-permute-start(bf16[256,2048]{1,0:T(8,128)(2,1)} %param.19), channel_id=1, source_target_pairs={{0,16},{16,0},{1,17},{17,1},{2,18},{18,2},{3,19},{19,3},{4,20},{20... | collective-permute-start | bytes 3145736 | tf_op jit(solution)/shard_map/ppermute | solution.py:13
  29.5 1.0 convert_reduce_fusion
  30.4 1.1 copy.33
  32.1 2.3 convolution_bitcast_fusion
  34.4 0.7 all-to-all-done
  35.1 0.7 fusion.104
  35.8 0.1 reduce.2
  36.0 1.2 select_add_fusion.2
  37.2 0.1 select_reduce_fusion.5
  37.3 1.5 fusion.27
  38.9 0.0 copy-start.5
  38.9 0.0 copy-start.10
  38.9 0.1 copy.34
  39.0 0.1 reshape.272
  39.1 0.7 copy.35
  39.8 3.4 %all-to-all-start.1 = ((bf16[2,4,64,256]{3,2,1,0:T(8,128)(2,1)}), bf16[2,4,64,256]{3,2,1,0:T(8,128)(2,1)S(1)}, u32[]{:S(2)}, u32[]{:S(2)}) async-start(bf16[2,4,64,256]{3,2,1,0:T(8,128)(2,1)} %copy.35), calls=%async_computation.1 | async-start | bytes 524288 | tf_op jit(solution)/shard_map/all_to_all | solution.py:141
  43.3 0.1 slice_subtract_fusion.1
  43.4 0.2 select_reduce_fusion.1
  43.6 4.9 %all-to-all-done.1 = bf16[2,4,64,256]{3,2,1,0:T(8,128)(2,1)S(1)} async-done(((bf16[2,4,64,256]{3,2,1,0:T(8,128)(2,1)}), bf16[2,4,64,256]{3,2,1,0:T(8,128)(2,1)S(1)}, u32[]{:S(2)}, u32[]{:S(2)}) %all-to-all-start.1) | async-done | bytes 262176 | tf_op jit(solution)/shard_map/all_to_all | solution.py:141
  48.5 0.2 fusion.87
  48.7 0.2 fusion.89
  48.9 0.2 fusion.91
  49.1 0.2 fusion.93
  49.4 0.1 fusion.45
  49.5 22.5 %collective-permute-start.5 = (bf16[256,512]{0,1:T(8,128)(2,1)S(1)}, bf16[256,512]{0,1:T(8,128)(2,1)S(1)}, u32[]{:S(2)}, u32[]{:S(2)}) collective-permute-start(bf16[256,512]{0,1:T(8,128)(2,1)S(1)} %fusion.45), channel_id=1, source_target_pairs={{0,16},{16,0},{1,17},{17,1},{2,18},{18,2},{3,19},{19,3},{4,20},{20... | collective-permute-start | bytes 786440 | tf_op jit(solution)/shard_map/ppermute | solution.py:13
  72.0 0.8 multiply_reduce_fusion.4
  72.9 16.7 %collective-permute-done.5 = bf16[256,512]{0,1:T(8,128)(2,1)S(1)} collective-permute-done((bf16[256,512]{0,1:T(8,128)(2,1)S(1)}, bf16[256,512]{0,1:T(8,128)(2,1)S(1)}, u32[]{:S(2)}, u32[]{:S(2)}) %collective-permute-start.5) | collective-permute-done | bytes 262176 | tf_op jit(solution)/shard_map/ppermute | solution.py:13
  89.6 0.8 multiply_reduce_fusion.2
  90.4 2.4 multiply_reduce_fusion.1
  92.8 3.7 %convolution_convert_fusion = bf16[512,2048]{1,0:T(8,128)(2,1)} fusion(f32[256,2048]{1,0:T(8,128)S(1)} %get-tuple-element.40, bf16[256,2048]{1,0:T(8,128)(2,1)} %collective-permute-done.4, f32[256]{0:T(256)S(1)} %get-tuple-element.45, f32[256]{0:T(256)S(1)} %add_rsqrt_fusion.2, f32[2048]{0:T(1024)S(1)} %copy-done.11, f32[2048]{0:T(1024)S(1)} %copy-done.7, ...), kind=kOutput, calls=%fused_computation.14 | convolution fusion | flops 542507008 | bytes 5263360 | tf_op jit(solution)/shard_map/dot_general | solution.py:26
  96.5 4.4 %all-to-all-start.4 = ((bf16[16,32,2048]{2,1,0:T(8,128)(2,1)}), bf16[16,32,2048]{2,1,0:T(8,128)(2,1)}, u32[]{:S(2)}, u32[]{:S(2)}) async-start(bf16[16,32,2048]{2,1,0:T(8,128)(2,1)} %bitcast.121), calls=%async_computation.4 | async-start | bytes 4194304 | tf_op jit(solution)/shard_map/all_to_all | solution.py:165
  101.0 0.2 select_reduce_fusion.3
  101.2 4.0 %convolution_convert_fusion.1 = bf16[512,2048]{1,0:T(8,128)(2,1)} fusion(f32[256]{0:T(256)S(1)} %get-tuple-element.46, f32[2048]{0:T(1024)S(1)} %copy-done.11, f32[256]{0:T(256)S(1)} %broadcast_add_fusion.2, f32[256]{0:T(256)S(1)} %broadcast_add_fusion.3, f32[256,2048]{1,0:T(8,128)} %copy-done.1, bf16[256,2048]{1,0:T(8,128)(2,1)S(1)} %copy-done.3, ...), kind=kOutput, calls=%fused_computation.15 | convolution fusion | flops 542507008 | bytes 5263360 | tf_op jit(solution)/shard_map/dot_general | solution.py:26
  105.2 22.9 %all-to-all-done.4 = bf16[16,32,2048]{2,1,0:T(8,128)(2,1)} async-done(((bf16[16,32,2048]{2,1,0:T(8,128)(2,1)}), bf16[16,32,2048]{2,1,0:T(8,128)(2,1)}, u32[]{:S(2)}, u32[]{:S(2)}) %all-to-all-start.4) | async-done | bytes 2097184 | tf_op jit(solution)/shard_map/all_to_all | solution.py:165
  128.1 5.2 %all-to-all-start.2 = ((bf16[16,32,2048]{2,1,0:T(8,128)(2,1)}), bf16[16,32,2048]{2,1,0:T(8,128)(2,1)}, u32[]{:S(2)}, u32[]{:S(2)}) async-start(bf16[16,32,2048]{2,1,0:T(8,128)(2,1)} %bitcast.123), calls=%async_computation.2 | async-start | bytes 4194304 | tf_op jit(solution)/shard_map/all_to_all | solution.py:165
  133.3 6.5 %fusion.8 = f32[512,1024]{1,0:T(8,128)} fusion(bf16[512,2048]{1,0:T(8,128)(2,1)} %bitcast.39, bf16[1,2048,1024]{2,1,0:T(8,128)(2,1)} %param.25), kind=kOutput, calls=%fused_computation.8 | convolution fusion | flops 2147483648 | bytes 8388608 | tf_op jit(solution)/shard_map/dot_general | solution.py:26
  139.7 10.5 %fusion.15 = bf16[512,2048]{1,0:T(8,128)(2,1)} fusion(bf16[1,1024,2048]{2,1,0:T(8,128)(2,1)} %param.27, f32[512,1024]{1,0:T(8,128)} %fusion.8, bf16[512,2048]{1,0:T(8,128)(2,1)} %bitcast.39, bf16[1,2048,1024]{2,1,0:T(8,128)(2,1)} %param.26), kind=kOutput, calls=%fused_computation.13 | convolution fusion | flops 4299161600 | bytes 14680064 | tf_op jit(solution)/shard_map/dot_general | solution.py:26
  150.3 11.1 %all-to-all-done.2 = bf16[16,32,2048]{2,1,0:T(8,128)(2,1)} async-done(((bf16[16,32,2048]{2,1,0:T(8,128)(2,1)}), bf16[16,32,2048]{2,1,0:T(8,128)(2,1)}, u32[]{:S(2)}, u32[]{:S(2)}) %all-to-all-start.2) | async-done | bytes 2097184 | tf_op jit(solution)/shard_map/all_to_all | solution.py:165
  161.3 4.4 %all-to-all-start.5 = ((bf16[16,32,2048]{2,1,0:T(8,128)(2,1)}), bf16[16,32,2048]{2,1,0:T(8,128)(2,1)}, u32[]{:S(2)}, u32[]{:S(2)}) async-start(bf16[16,32,2048]{2,1,0:T(8,128)(2,1)} %bitcast.122), calls=%async_computation.5 | async-start | bytes 4194304 | tf_op jit(solution)/shard_map/all_to_all | solution.py:165
  165.8 6.5 %fusion.10 = f32[512,1024]{1,0:T(8,128)} fusion(bf16[512,2048]{1,0:T(8,128)(2,1)} %bitcast.28, bf16[1,2048,1024]{2,1,0:T(8,128)(2,1)} %param.25), kind=kOutput, calls=%fused_computation.10 | convolution fusion | flops 2147483648 | bytes 8388608 | tf_op jit(solution)/shard_map/dot_general | solution.py:26
  172.3 10.6 %fusion.12 = bf16[512,2048]{1,0:T(8,128)(2,1)} fusion(bf16[1,1024,2048]{2,1,0:T(8,128)(2,1)} %param.27, f32[512,1024]{1,0:T(8,128)} %fusion.10, bf16[512,2048]{1,0:T(8,128)(2,1)} %bitcast.28, bf16[1,2048,1024]{2,1,0:T(8,128)(2,1)} %param.26), kind=kOutput, calls=%fused_computation.12 | convolution fusion | flops 4299161600 | bytes 14680064 | tf_op jit(solution)/shard_map/dot_general | solution.py:26
  182.9 10.4 %all-to-all-done.5 = bf16[16,32,2048]{2,1,0:T(8,128)(2,1)} async-done(((bf16[16,32,2048]{2,1,0:T(8,128)(2,1)}), bf16[16,32,2048]{2,1,0:T(8,128)(2,1)}, u32[]{:S(2)}, u32[]{:S(2)}) %all-to-all-start.5) | async-done | bytes 2097184 | tf_op jit(solution)/shard_map/all_to_all | solution.py:165
  193.3 4.8 %all-to-all-start.3 = ((bf16[16,32,2048]{2,1,0:T(8,128)(2,1)}), bf16[16,32,2048]{2,1,0:T(8,128)(2,1)}, u32[]{:S(2)}, u32[]{:S(2)}) async-start(bf16[16,32,2048]{2,1,0:T(8,128)(2,1)} %bitcast.120), calls=%async_computation.3 | async-start | bytes 4194304 | tf_op jit(solution)/shard_map/all_to_all | solution.py:165
  198.1 2.4 fusion.55
  200.5 3.4 %fusion.18 = bf16[256,2048]{1,0:T(8,128)(2,1)} fusion(f32[256,2048]{1,0:T(8,128)S(1)} %fusion.55, bf16[512,2048]{1,0:T(8,128)(2,1)} %bitcast.41, f32[256]{0:T(256)S(1)} %bitcast.138, f32[256]{0:T(256)S(1)} %broadcast_add_fusion, f32[256]{0:T(256)S(1)} %bitcast.140, f32[256]{0:T(256)S(1)} %broadcast_add_fusion.1), kind=kOutput, calls=%fused_computation.18 | convolution fusion | flops 538968064 | bytes 5246976 | tf_op jit(solution)/shard_map/dot_general | solution.py:30
  203.9 0.9 collective-permute-start.6
  204.8 38.3 %all-to-all-done.3 = bf16[16,32,2048]{2,1,0:T(8,128)(2,1)} async-done(((bf16[16,32,2048]{2,1,0:T(8,128)(2,1)}), bf16[16,32,2048]{2,1,0:T(8,128)(2,1)}, u32[]{:S(2)}, u32[]{:S(2)}) %all-to-all-start.3) | async-done | bytes 2097184 | tf_op jit(solution)/shard_map/all_to_all | solution.py:165
  243.1 2.4 fusion.54
  245.5 7.4 %collective-permute-done.6 = bf16[256,2048]{1,0:T(8,128)(2,1)S(1)} collective-permute-done((bf16[256,2048]{1,0:T(8,128)(2,1)}, bf16[256,2048]{1,0:T(8,128)(2,1)S(1)}, u32[]{:S(2)}, u32[]{:S(2)}) %collective-permute-start.6) | collective-permute-done | bytes 1048608 | tf_op jit(solution)/shard_map/ppermute | solution.py:13
  252.9 2.6 %multiply_reduce_fusion = (f32[256]{0:T(256)S(1)}, f32[256,2048]{1,0:T(8,128)S(1)}) fusion(bf16[256,2048]{1,0:T(8,128)(2,1)S(1)} %collective-permute-done.6, f32[256,2048]{1,0:T(8,128)S(1)} %fusion.54, bf16[512,2048]{1,0:T(8,128)(2,1)} %bitcast.33, f32[256]{0:T(256)S(1)} %bitcast.136, f32[256]{0:T(256)S(1)} %broadcast_add_fusion.2, f32[256]{0:T(256)S(1)} %bitcast.134, ...), kind=kOutput, calls=%fused_computation.20 | convolution fusion | flops 540540672 | bytes 7345152 | tf_op jit(solution)/shard_map/dot_general | solution.py:30
  255.6 1.8 add_convert_fusion
  (45 shorter events, 0.3 us)
Async XLA Ops:
  0.0 72.0 %copy-start = (bf16[512,2048]{1,0:T(8,128)(2,1)S(1)}, bf16[512,2048]{1,0:T(8,128)(2,1)}, u32[]{:S(2)}) copy-start(bf16[512,2048]{1,0:T(8,128)(2,1)} %param.18) | copy-start | bytes 6291460
  0.0 36.0 %copy-start.6 = (s32[512]{0:T(512)S(1)}, s32[512]{0:T(512)}, u32[]{:S(2)}) copy-start(s32[512]{0:T(512)} %param.15) | copy-start | bytes 6148
  1.1 36.2 %collective-permute-start.3 = (bf16[64,512]{1,0:T(8,128)(2,1)S(1)}, bf16[64,512]{1,0:T(8,128)(2,1)S(1)}, u32[]{:S(2)}, u32[]{:S(2)}) collective-permute-start(bf16[64,512]{1,0:T(8,128)(2,1)S(1)} %get-tuple-element.25), channel_id=1, source_target_pairs={{0,16},{2,18},{4,20},{6,22},{8,24},{10,26},{12,28},{14,30},{1,17},... | collective-permute-start | bytes 196616 | tf_op jit(solution)/shard_map/ppermute | solution.py:18
  7.1 30.2 %collective-permute-start.2 = (bf16[64,512]{1,0:T(8,128)(2,1)S(1)}, bf16[64,512]{1,0:T(8,128)(2,1)S(1)}, u32[]{:S(2)}, u32[]{:S(2)}) collective-permute-start(bf16[64,512]{1,0:T(8,128)(2,1)S(1)} %get-tuple-element.26), channel_id=1, source_target_pairs={{0,8},{2,10},{4,12},{6,14},{8,16},{10,18},{12,20},{14,22},{16,24},... | collective-permute-start | bytes 196616 | tf_op jit(solution)/shard_map/ppermute | solution.py:18
  10.6 26.7 %collective-permute-start.1 = (bf16[64,512]{1,0:T(8,128)(2,1)S(1)}, bf16[64,512]{1,0:T(8,128)(2,1)S(1)}, u32[]{:S(2)}, u32[]{:S(2)}) collective-permute-start(bf16[64,512]{1,0:T(8,128)(2,1)S(1)} %get-tuple-element.24), channel_id=1, source_target_pairs={{0,4},{2,6},{4,8},{6,10},{8,12},{10,14},{12,16},{14,18},{16,20},{1... | collective-permute-start | bytes 196616 | tf_op jit(solution)/shard_map/ppermute | solution.py:18
  14.0 23.3 %collective-permute-start = (bf16[64,512]{1,0:T(8,128)(2,1)S(1)}, bf16[64,512]{1,0:T(8,128)(2,1)S(1)}, u32[]{:S(2)}, u32[]{:S(2)}) collective-permute-start(bf16[64,512]{1,0:T(8,128)(2,1)S(1)} %get-tuple-element.23), channel_id=1, source_target_pairs={{0,2},{2,4},{4,6},{6,8},{8,10},{10,12},{12,14},{14,16},{16,18},{18... | collective-permute-start | bytes 196616 | tf_op jit(solution)/shard_map/ppermute | solution.py:18
  23.1 12.0 %all-to-all-start = ((f32[16,16,128]{2,1,0:T(8,128)}), f32[16,16,128]{2,1,0:T(8,128)S(1)}, u32[]{:S(2)}, u32[]{:S(2)}) async-start(f32[16,16,128]{2,1,0:T(8,128)} %broadcast_in_dim.138), calls=%async_computation | async-start | bytes 262144 | tf_op jit(solution)/shard_map/all_to_all | solution.py:112
  26.7 63.7 %collective-permute-start.4 = (bf16[256,2048]{1,0:T(8,128)(2,1)}, bf16[256,2048]{1,0:T(8,128)(2,1)}, u32[]{:S(2)}, u32[]{:S(2)}) collective-permute-start(bf16[256,2048]{1,0:T(8,128)(2,1)} %param.19), channel_id=1, source_target_pairs={{0,16},{16,0},{1,17},{17,1},{2,18},{18,2},{3,19},{19,3},{4,20},{20... | collective-permute-start | bytes 3145736 | tf_op jit(solution)/shard_map/ppermute | solution.py:13
  38.9 9.6 %copy-start.5 = (bf16[4,128,128]{2,1,0:T(8,128)(2,1)S(1)}, bf16[4,128,128]{2,1,0:T(8,128)(2,1)}, u32[]{:S(2)}) copy-start(bf16[4,128,128]{2,1,0:T(8,128)(2,1)} %param.16) | copy-start | bytes 393220
  38.9 10.5 %copy-start.10 = (f32[512]{0:T(512)S(1)}, f32[512]{0:T(512)}, u32[]{:S(2)}) copy-start(f32[512]{0:T(512)} %param.17) | copy-start | bytes 6148
  39.8 8.6 %all-to-all-start.1 = ((bf16[2,4,64,256]{3,2,1,0:T(8,128)(2,1)}), bf16[2,4,64,256]{3,2,1,0:T(8,128)(2,1)S(1)}, u32[]{:S(2)}, u32[]{:S(2)}) async-start(bf16[2,4,64,256]{3,2,1,0:T(8,128)(2,1)} %copy.35), calls=%async_computation.1 | async-start | bytes 524288 | tf_op jit(solution)/shard_map/all_to_all | solution.py:141
  49.5 40.1 %collective-permute-start.5 = (bf16[256,512]{0,1:T(8,128)(2,1)S(1)}, bf16[256,512]{0,1:T(8,128)(2,1)S(1)}, u32[]{:S(2)}, u32[]{:S(2)}) collective-permute-start(bf16[256,512]{0,1:T(8,128)(2,1)S(1)} %fusion.45), channel_id=1, source_target_pairs={{0,16},{16,0},{1,17},{17,1},{2,18},{18,2},{3,19},{19,3},{4,20},{20... | collective-permute-start | bytes 786440 | tf_op jit(solution)/shard_map/ppermute | solution.py:13
  72.8 17.6 %copy-start.1 = (f32[256,2048]{1,0:T(8,128)}, f32[256,2048]{1,0:T(8,128)S(1)}, u32[]{:S(2)}) copy-start(f32[256,2048]{1,0:T(8,128)S(1)} %get-tuple-element.42) | copy-start | bytes 6291460
  72.8 17.6 %copy-start.3 = (bf16[256,2048]{1,0:T(8,128)(2,1)S(1)}, bf16[256,2048]{1,0:T(8,128)(2,1)}, u32[]{:S(2)}) copy-start(bf16[256,2048]{1,0:T(8,128)(2,1)} %param.19) | copy-start | bytes 3145732
  72.8 17.6 %copy-start.7 = (f32[2048]{0:T(1024)S(1)}, f32[2048]{0:T(1024)}, u32[]{:S(2)}) copy-start(f32[2048]{0:T(1024)} %param.20) | copy-start | bytes 24580
  90.4 2.4 copy-start.11
  96.5 31.5 %all-to-all-start.4 = ((bf16[16,32,2048]{2,1,0:T(8,128)(2,1)}), bf16[16,32,2048]{2,1,0:T(8,128)(2,1)}, u32[]{:S(2)}, u32[]{:S(2)}) async-start(bf16[16,32,2048]{2,1,0:T(8,128)(2,1)} %bitcast.121), calls=%async_computation.4 | async-start | bytes 4194304 | tf_op jit(solution)/shard_map/all_to_all | solution.py:165
  128.1 33.3 %all-to-all-start.2 = ((bf16[16,32,2048]{2,1,0:T(8,128)(2,1)}), bf16[16,32,2048]{2,1,0:T(8,128)(2,1)}, u32[]{:S(2)}, u32[]{:S(2)}) async-start(bf16[16,32,2048]{2,1,0:T(8,128)(2,1)} %bitcast.123), calls=%async_computation.2 | async-start | bytes 4194304 | tf_op jit(solution)/shard_map/all_to_all | solution.py:165
  161.3 31.9 %all-to-all-start.5 = ((bf16[16,32,2048]{2,1,0:T(8,128)(2,1)}), bf16[16,32,2048]{2,1,0:T(8,128)(2,1)}, u32[]{:S(2)}, u32[]{:S(2)}) async-start(bf16[16,32,2048]{2,1,0:T(8,128)(2,1)} %bitcast.122), calls=%async_computation.5 | async-start | bytes 4194304 | tf_op jit(solution)/shard_map/all_to_all | solution.py:165
  193.3 49.9 %all-to-all-start.3 = ((bf16[16,32,2048]{2,1,0:T(8,128)(2,1)}), bf16[16,32,2048]{2,1,0:T(8,128)(2,1)}, u32[]{:S(2)}, u32[]{:S(2)}) async-start(bf16[16,32,2048]{2,1,0:T(8,128)(2,1)} %bitcast.120), calls=%async_computation.3 | async-start | bytes 4194304 | tf_op jit(solution)/shard_map/all_to_all | solution.py:165
  200.5 4.3 %copy-start.8 = (f32[256,2]{0,1:T(2,128)S(1)}, f32[256,2]{0,1:T(2,128)}, u32[]{:S(2)}) copy-start(f32[256,2]{0,1:T(2,128)} %param.24) | copy-start | bytes 6148
  203.9 49.0 %collective-permute-start.6 = (bf16[256,2048]{1,0:T(8,128)(2,1)}, bf16[256,2048]{1,0:T(8,128)(2,1)S(1)}, u32[]{:S(2)}, u32[]{:S(2)}) collective-permute-start(bf16[256,2048]{1,0:T(8,128)(2,1)} %fusion.18), channel_id=1, source_target_pairs={{0,16},{16,0},{1,17},{17,1},{2,18},{18,2},{3,19},{19,3},{4,20},{20... | collective-permute-start | bytes 3145736 | tf_op jit(solution)/shard_map/ppermute | solution.py:13
  245.5 10.1 %copy-start.2 = (f32[256,2048]{1,0:T(8,128)S(1)}, f32[256,2048]{1,0:T(8,128)}, u32[]{:S(2)}) copy-start(f32[256,2048]{1,0:T(8,128)} %copy-done.1) | copy-start | bytes 6291460
  245.5 10.1 %copy-start.4 = (bf16[256,2048]{1,0:T(8,128)(2,1)S(1)}, bf16[256,2048]{1,0:T(8,128)(2,1)}, u32[]{:S(2)}) copy-start(bf16[256,2048]{1,0:T(8,128)(2,1)} %param.19) | copy-start | bytes 3145732
  245.5 10.1 %copy-start.9 = (f32[2048]{0:T(1024)S(1)}, f32[2048]{0:T(1024)}, u32[]{:S(2)}) copy-start(f32[2048]{0:T(1024)} %param.22) | copy-start | bytes 24580

commit v2 on v1

v2 whole, which is shorter than its diff:
```python
import functools
import math

import jax
import jax.numpy as jnp
from jax import lax
from jax.experimental import pallas as pl
from jax.experimental.pallas import tpu as pltpu
from jax.sharding import Mesh, PartitionSpec as P


BF16, F32 = jnp.bfloat16, jnp.float32
SP = ("zh", "zl", "yc")
HALF = ("zl", "yc", "tp")
ALL = ("zh", "zl", "yc", "tp")
LANES = 128
PIECES = 3
VM = pl.BlockSpec(memory_space=pltpu.VMEM)
SM = pl.BlockSpec(memory_space=pltpu.SMEM)


def in_hbm(x):
    return pltpu.with_memory_space_constraint(x, pltpu.HBM)


def to_twin(x, inner=True, outer=True):
    last = 2 * lax.axis_size("zl") - 1
    places = range(last + 1)
    used = [i for i in places if (outer if i in (0, last) else inner)]
    return (lax.ppermute(x, ("zh", "zl"), [(i, last - i) for i in used]))


def passed_along(x, by):
    devices = lax.axis_size("zh") * lax.axis_size("zl") * lax.axis_size("yc")
    return (lax.ppermute(x, SP, [(i, i + by) for i in range(devices - by)]))


def rms_scale(vector):
    return lax.rsqrt(jnp.mean(vector * vector, axis=-1, keepdims=True) + 1e-06)


def dot(a, b):
    return jnp.dot(a, b, preferred_element_type=F32)


def dot_t(a, b):
    return lax.dot_general(a, b, (((0,), (0,)), ((), ())), preferred_element_type=F32)


def dot_nt(a, b):
    return lax.dot_general(a, b, (((1,), (1,)), ((), ())), preferred_element_type=F32)


def iota(shape, dim):
    return lax.broadcasted_iota(jnp.int32, shape, dim)


def column(row):
    return jnp.transpose(jnp.broadcast_to(row, (8, row.shape[1])))[:, :1]


def call(kernel, outs, *args, vmem=16 * 2**20, flops=0):
    specs = [SM if a.ndim == 1 else VM for a in args]
    shapes = [(pltpu.HBM if where else jax.ShapeDtypeStruct)(s, d) for s, d, *where in outs]
    moved = sum(a.size * a.dtype.itemsize for a in args)
    moved += sum(math.prod(s) * jnp.dtype(d).itemsize for s, d, *_ in outs)
    return pl.pallas_call(
        kernel,
        out_shape=shapes,
        in_specs=specs,
        out_specs=[VM] * len(shapes),
        compiler_params=pltpu.CompilerParams(vmem_limit_bytes=vmem),
        cost_estimate=pl.CostEstimate(flops=flops, transcendentals=0, bytes_accessed=moved),
    )(*args)


def head_kernel(x_ref, docs_ref, ids_ref, logits_ref, res_ref, news_ref, *refs):
    groups, channels, length = x_ref.shape
    block_refs, piece_refs = refs[:groups], refs[groups:]
    part = piece_refs[0].shape[0]
    piece_refs[0][...] = res_ref[:part]
    piece_refs[1][...] = res_ref[part:]
    piece_refs[2][...] = res_ref[...]
    blocks = news_ref.shape[0]
    docs = docs_ref[...]
    tail = docs == docs[:, length - 1 :]
    flat = x_ref[...].reshape(groups * channels, length)
    tails = jnp.broadcast_to(jnp.where(tail, 1.0, 0.0), (8, length)).astype(BF16)
    sums = dot_nt(tails, flat)[:1]
    count = jnp.sum(jnp.where(tail, 1.0, 0.0), axis=1, keepdims=True)
    wide = (1, LANES)
    lines = [sums[:, i : i + LANES] for i in range(0, groups * channels, LANES)]
    lines.append(jnp.broadcast_to(count, wide))
    lines.append(jnp.broadcast_to(docs[:, length - 1 :].astype(F32), wide))
    rows = ids_ref.shape[1]
    for ref in (ids_ref, logits_ref):
        for k in range(2):
            line = ref[k : k + 1].astype(F32)
            lines += [line[:, i : i + LANES] for i in range(0, rows, LANES)]
    spare = news_ref.shape[1] - len(lines)
    lines.append(jnp.zeros((spare, LANES), F32))
    payload = jnp.concatenate(lines, axis=0)
    for b in range(blocks):
        news_ref[b] = payload
    for g in range(groups):
        block_refs[g][...] = x_ref[g]


def pool_kernel(where_ref, x_ref, docs_ref, news_ref, *refs):
    groups, channels, length = x_ref.shape
    far_refs, out_refs = refs[:groups], refs[groups:]
    tp, rows = len(out_refs), out_refs[0].shape[2]
    mine = where_ref[0]
    width = groups * channels
    lines = width // LANES
    docs = docs_ref[...]
    first_doc = docs == docs[:, :1]
    block = iota((news_ref.shape[0], LANES), 0)
    joins = (block < mine) & (news_ref[:, lines + 1, :] == docs[:, :1].astype(F32))
    earlier = jnp.sum(jnp.where(joins, news_ref[:, lines, :], 0.0), axis=0, keepdims=True)[:, :1]
    carries, betweens = [], []
    for i in range(lines):
        sums = news_ref[:, i, :]
        reach = 1 << ((iota(sums.shape, 1) + i * LANES) // channels)
        inside = (block < mine) & (block > mine - reach)
        carries.append(jnp.sum(jnp.where(joins, sums, 0.0), axis=0, keepdims=True))
        betweens.append(jnp.sum(jnp.where(inside, sums, 0.0), axis=0, keepdims=True))
    carry = column(jnp.concatenate(carries, axis=1))
    between = column(jnp.concatenate(betweens, axis=1))
    down, across = iota((length, length), 0), iota((length, length), 1)
    docs_f = docs.astype(F32)
    within = (down <= across) & (column(docs_f) == docs_f)
    within = jnp.where(within, 1.0, 0.0)
    position = jnp.sum(within, axis=0, keepdims=True) + jnp.where(first_doc, earlier, 0.0)
    within = within.astype(BF16)
    after = jnp.where(down > across, 1.0, 0.0).astype(BF16)
    for g in range(groups):
        x = x_ref[g]
        part = slice(g * channels, (g + 1) * channels)
        span = float(length * 2**g)
        near = dot(x, within)
        far = dot(far_refs[g][...], after)
        begun = jnp.where(first_doc, carry[part], 0.0)
        window = near + jnp.where(position > span, between[part] + far, begun)
        diff = (window / jnp.minimum(position, span) - x.astype(F32)).astype(BF16)
        for j in range(tp):
            for away in range(tp):

                @pl.when(where_ref[3] == (j - away) % tp)
                def _():
                    out_refs[away][g] = diff[:, j * rows : (j + 1) * rows]


def map_kernel(where_ref, maps_ref, scale_ref, *refs):
    d_refs, out_ref = refs[:-1], refs[-1]
    tp, (groups, channels, rows) = len(d_refs), d_refs[0].shape
    wide = maps_ref.shape[2]
    for g in range(groups):
        total = jnp.zeros((rows, wide), F32)
        for away in range(tp):
            source = lax.rem(where_ref[3] + tp - away, tp)
            start = pl.multiple_of(source * channels, channels)
            total += dot_t(d_refs[away][g], maps_ref[g, pl.ds(start, channels)])
        part = slice(g * wide, (g + 1) * wide)
        out_ref[:, part] = (total * scale_ref[:, part]).astype(BF16)


def slots_of(ids, first, experts, capacity):
    rows = ids[0].shape[1]
    expert = iota((experts, rows), 0).astype(F32)
    named = [i - first == expert for i in ids]
    held = jnp.where(named[0] | named[1], 1.0, 0.0).astype(BF16)
    earlier = jnp.where(iota((rows, rows), 0) < iota((rows, rows), 1), 1.0, 0.0).astype(BF16)
    place = dot(held, earlier) + expert * float(capacity) + 1.0
    return [jnp.sum(jnp.where(n, place, 0.0), axis=0, keepdims=True) - 1.0 for n in named]


def read_routes(where_ref, news_ref, skip, rows):
    at, step = where_ref[1], rows // LANES
    out = []
    for k in range(4):
        out.append(
            jnp.concatenate(
                [news_ref[at, pl.ds(skip + k * step + i, 1), :] for i in range(step)], axis=1
            )
        )
    return out[:2], out[2:]


def table_kernel(capacity, skip, where_ref, news_ref, pick_ref, weight_ref):
    slots, rows = pick_ref.shape
    experts = slots // capacity
    ids, logits = read_routes(where_ref, news_ref, skip, rows)
    at = slots_of(ids, where_ref[2].astype(F32), experts, capacity)
    slot = iota((slots, rows), 0).astype(F32)
    pick_ref[...] = jnp.where((slot == at[0]) | (slot == at[1]), 1.0, 0.0).astype(BF16)
    weights = [jax.nn.sigmoid(logits[0] - logits[1]), jax.nn.sigmoid(logits[1] - logits[0])]
    slot = iota((rows, slots), 1).astype(F32)
    weight = jnp.zeros((rows, slots), F32)
    for k in range(2):
        weight = jnp.where(slot == column(at[k]), column(weights[k]), weight)
    weight_ref[...] = weight.astype(BF16)


def send_kernel(where_ref, mapped_ref, w_ref, mix_ref, ffn_ref, pick_ref, *refs):
    n = 1 if refs[0].shape[0] == mapped_ref.shape[0] else PIECES
    res_refs, send_ref, stream_refs = refs[:n], refs[n], refs[n + 1 :]
    projected = dot(mapped_ref[...], w_ref[...])
    residual = res_refs[-1][...]
    if n > 1:
        outer = jnp.concatenate([r[...] for r in res_refs[:-1]], axis=0)
        residual = jnp.where(where_ref[4] == 1, outer, residual)
    stream = residual.astype(F32) + mix_ref[...] * projected * rms_scale(projected)
    stream = stream.astype(BF16)
    if stream_refs:
        stream_refs[0][...] = stream
    stream = stream.astype(F32)
    normed = (ffn_ref[...] * stream * rms_scale(stream)).astype(BF16)
    send_ref[...] = dot(pick_ref[...], normed).astype(BF16)


def sum_kernel(weight_ref, back_ref, out_ref):
    out_ref[...] = dot(weight_ref[...], back_ref[...]).astype(out_ref.dtype)


def last_kernel(own_0, own_1, other_0, other_1, stream_ref, gain_ref, out_ref):
    total = jnp.concatenate(
        [own_0[...] + other_0[...].astype(F32), own_1[...] + other_1[...].astype(F32)], axis=1
    )
    out = stream_ref[...].astype(F32) + gain_ref[...] * total * rms_scale(total)
    out_ref[...] = out.astype(BF16)


def expert_kernel(tiles, x_ref, gate_ref, up_ref, down_ref, *refs):
    out_refs, hidden_ref = refs[:-1], refs[-1]
    step = pl.program_id(0)
    tile = gate_ref.shape[2]

    @pl.when(step < tiles)
    def _():
        x = x_ref[...]
        gate, up = dot(x, gate_ref[0]), dot(x, up_ref[0])
        hidden = (gate / (1.0 + jnp.exp(-gate)) * up).astype(BF16)
        hidden_ref[:, pl.ds(pl.multiple_of(step * tile, tile), tile)] = hidden

    for i, out_ref in enumerate(out_refs):

        @pl.when(step == tiles + i)
        def _():
            out_ref[...] = dot(hidden_ref[...], down_ref[0]).astype(BF16)


def expert_rows(x, w_gate, w_up, w_down, parts, columns):
    n, width = x.shape
    inner = w_gate.shape[2]
    tile = min(inner, 512)
    tiles = inner // tile
    early = lambda i: (0, 0, jnp.minimum(i, tiles - 1))
    whole = lambda i: (0, 0)
    return pl.pallas_call(
        functools.partial(expert_kernel, tiles),
        grid=(tiles + parts,),
        out_shape=[pltpu.HBM((n, columns), BF16)] * parts + [pltpu.HBM((n, inner), BF16)],
        in_specs=[
            pl.BlockSpec((n, width), whole),
            pl.BlockSpec((1, width, tile), early),
            pl.BlockSpec((1, width, tile), early),
            pl.BlockSpec((1, inner, columns), lambda i: (0, 0, jnp.maximum(i - tiles, 0))),
        ],
        out_specs=[pl.BlockSpec((n, columns), whole)] * parts + [pl.BlockSpec((n, inner), whole)],
        compiler_params=pltpu.CompilerParams(
            dimension_semantics=("arbitrary",), vmem_limit_bytes=32 * 2**20
        ),
        cost_estimate=pl.CostEstimate(
            flops=2 * n * inner * (2 * width + parts * columns),
            transcendentals=n * inner,
            bytes_accessed=2 * inner * (2 * width + parts * columns) + 4 * n * width,
        ),
    )(x, w_gate, w_up, w_down)


def down_kernel(hidden_ref, down_ref, out_ref):
    out_ref[...] = dot(hidden_ref[...], down_ref[0]).astype(BF16)


def down_rows(hidden, w_down, start):
    n, inner = hidden.shape
    columns = w_down.shape[2] - start
    tile = min(columns, 1024)
    skip = start // tile
    return pl.pallas_call(
        down_kernel,
        grid=(columns // tile,),
        out_shape=pltpu.HBM((n, columns), BF16),
        in_specs=[
            pl.BlockSpec((n, inner), lambda i: (0, 0)),
            pl.BlockSpec((1, inner, tile), lambda i: (0, 0, i + skip)),
        ],
        out_specs=pl.BlockSpec((n, tile), lambda i: (0, i)),
        compiler_params=pltpu.CompilerParams(vmem_limit_bytes=32 * 2**20),
        cost_estimate=pl.CostEstimate(
            flops=2 * n * inner * columns,
            transcendentals=0,
            bytes_accessed=2 * inner * (columns + n) + 2 * n * columns,
        ),
    )(hidden, w_down)


def local(
    pool_input,
    doc_ids,
    pool_map,
    pool_scale,
    w_out,
    residual,
    mix_gain,
    ffn_gain,
    out_gain,
    expert_ids,
    route_logits,
    *expert_weights,
):
    w_gate, w_up, w_down = [
        pltpu.with_memory_space_constraint(w, pltpu.HBM) for w in expert_weights
    ]
    groups, channels, length = pool_input.shape
    tp, planes, plane = lax.axis_size("tp"), lax.axis_size("zl"), lax.axis_size("yc")
    blocks = 2 * planes * plane
    rows, width = residual.shape
    experts = w_gate.shape[0] * planes * plane * tp
    capacity = max(2, rows * expert_ids.shape[1] // experts)
    slots = experts * capacity
    half, mine = lax.axis_index("zh"), lax.axis_index(SP)
    level = lax.axis_index(("zh", "zl"))
    twin = (2 * planes - 1 - level) * plane + lax.axis_index("yc")
    edge = ((level == 0) | (level == 2 * planes - 1)).astype(jnp.int32)
    first = half * experts
    column_at = lax.axis_index("tp")
    own_at = jnp.stack([mine, mine, first, column_at, edge])
    far_at = jnp.stack([mine, twin, first, column_at, edge])
    docs = in_hbm(doc_ids.reshape(1, length))
    pool_input, residual = in_hbm(pool_input), in_hbm(residual)
    skip = groups * channels // LANES + 2
    lines = skip + 4 * rows // LANES
    lines += -lines % 8
    sizes = (rows // 2, rows // 2, rows)
    news, *own_blocks = call(
        head_kernel,
        [((blocks, lines, LANES), F32)]
        + [((channels, length), BF16)] * groups
        + [((n, width), BF16, True) for n in sizes],
        pool_input,
        docs,
        in_hbm(expert_ids.T),
        in_hbm(route_logits.T),
        residual,
    )
    own_blocks, pieces = own_blocks[:groups], own_blocks[groups:]
    news = (lax.all_to_all(news, SP, 0, 0, tiled=True))
    far_blocks = []
    for g in range(groups):
        far_blocks.append(passed_along(own_blocks[g], 2**g))
    far_pieces = []
    for i in range(PIECES):
        far_pieces.append(to_twin(pieces[i], inner=i == 2, outer=i < 2))
    diffs = call(
        pool_kernel,
        [((groups, channels, rows), BF16)] * tp,
        own_at,
        pool_input,
        docs,
        news,
        *far_blocks,
    )
    diffs = list(diffs)
    for away in range(1, tp):
        turn = [(i, (i + away) % tp) for i in range(tp)]
        diffs[away] = (lax.ppermute(diffs[away], "tp", turn))
    (mapped,) = call(
        map_kernel,
        [((rows, groups * pool_map.shape[2]), BF16)],
        own_at,
        in_hbm(pool_map),
        in_hbm(pool_scale.reshape(1, -1)),
        *diffs,
    )
    far_mapped = to_twin(mapped)
    gains = (in_hbm(mix_gain.reshape(1, -1)), in_hbm(ffn_gain.reshape(1, -1)))
    table = functools.partial(table_kernel, capacity, skip)
    tables = [((slots, rows), BF16), ((rows, slots), BF16, True)]
    own_pick, own_weight = call(table, tables, own_at, news)
    far_pick, far_weight = call(table, tables, far_at, news)

    def there(x):
        columns = x.shape[1]
        x = x.reshape(experts, capacity, columns)
        return (lax.all_to_all(x, HALF, 0, 0, tiled=True).reshape(-1, columns))

    big = 24 * 2**20
    own_send, stream = call(
        send_kernel,
        [((slots, width), BF16, True), ((rows, width), BF16, True)],
        own_at, mapped, w_out, *gains, own_pick, residual,
        vmem=big,
    )
    own_in = there(own_send)
    (far_send,) = call(
        send_kernel,
        [((slots, width), BF16, True)],
        far_at, far_mapped, w_out, *gains, far_pick, *far_pieces,
        vmem=big,
    )
    far_in = there(far_send)
    part = width // 2
    *own_outs, _ = expert_rows(own_in, w_gate, w_up, w_down, 2, part)
    far_out_0, far_hidden = expert_rows(far_in, w_gate, w_up, w_down, 1, part)
    far_out_1 = down_rows(far_hidden, w_down, part)
    others, own_sums = [], []
    for outs in zip((far_out_0, far_out_1), own_outs):
        far_back = there(outs[0])
        (far_part,) = call(
            sum_kernel,
            [((rows, part), BF16)],
            far_weight, far_back,
            vmem=big,
        )
        others.append(to_twin(far_part))
        own_back = there(outs[1])
        own_sums += call(
            sum_kernel,
            [((rows, part), F32)],
            own_weight, own_back,
            vmem=big,
        )
    (out,) = call(
        last_kernel,
        [((rows, width), BF16)],
        *own_sums, *others, stream, in_hbm(out_gain.reshape(1, -1)),
        vmem=big,
    )
    return out


def solution(mesh):
    sp, tp = mesh.shape["sp"], mesh.shape["tp"]
    planes = 2 if sp % 4 == 0 else 1
    fine = Mesh(mesh.devices.reshape(2, planes, sp // (2 * planes), tp), ALL)
    rowwise = P(ALL, None)
    each = P(ALL, None, None)
    in_specs = (
        P(None, "tp", SP),
        P(SP),
        P(),
        P(),
        P(),
        rowwise,
        P(),
        P(),
        P(),
        rowwise,
        rowwise,
        each,
        each,
        each,
    )

    return jax.shard_map(local, mesh=fine, in_specs=in_specs, out_specs=rowwise, check_vma=False)
```

time: 258 us -> 256 us (level)
  the two profiles are of different devices: /device:TPU:0 before, /device:TPU:8 now
where the time goes in v2:
time: 256 us; the launch traced here: 255 us
  waiting for transfers between devices  124 us (48%)
  starting transfers between devices  56.6 us (22%)
  Pallas kernels  55.1 us (22%)
  blocking collectives  18.3 us (7%)
    ppermute x6, waiting for transfers between devices, to_twin(): return lax.ppermute(x, ('zh', 'zl'), [(i, last - i) for i in used])  87.7 us
    all_to_all x5, waiting for transfers between devices, there(): return lax.all_to_all(x, HALF, 0, 0, tiled=True).reshape(-1, columns)  33 us
    all_to_all x5, starting transfers between devices, there(): return lax.all_to_all(x, HALF, 0, 0, tiled=True).reshape(-1, columns)  28.8 us
    pallas_call x12, Pallas kernels, call(): pl.pallas_call(kernel, out_shape=shapes, in_specs=specs, out_specs=[VM] *...  27.6 us
    pallas_call x2, Pallas kernels, expert_rows(): pl.pallas_call(functools.partial(expert_kernel, tiles), grid=(tiles + par...  23.7 us
    all_to_all x1, blocking collectives, there(): return lax.all_to_all(x, HALF, 0, 0, tiled=True).reshape(-1, columns)  18.3 us
    ppermute x4, starting transfers between devices, passed_along(): return lax.ppermute(x, SP, [(i, i + by) for i in range(devices - by)])  10.9 us
    ppermute x6, starting transfers between devices, to_twin(): return lax.ppermute(x, ('zh', 'zl'), [(i, last - i) for i in used])  8.99 us
  transfers between devices with their start and end apart: 17, of which 10 were waited for; matrix products, arithmetic and copies ran while one was open for 0% of the time, Pallas kernels for 16%

profile of v2, /device:TPU:8, one launch (start us, length us, event | category | flops | bytes accessed | tf_op | source)
XLA Modules:
  0.0 255.5 jit_solution(7922934823516104573)
XLA Ops:
  0.0 0.0 copy-start
  0.0 2.9 %shard_map.136 = (f32[16,16,128]{2,1,0:T(8,128)}, bf16[64,512]{1,0:T(8,128)(2,1)S(1)}, bf16[64,512]{1,0:T(8,128)(2,1)S(1)}, bf16[64,512]{1,0:T(8,128)(2,1)S(1)},...) custom-call(bf16[4,64,512]{2,1,0:T(8,128)(2,1)} %x_ref.3, ...), custom_call_target="tpu_custom_call" | custom-call | bytes 3807232 | tf_op jit(solution)/shard_map/pallas_call | solution.py:67
  2.9 6.3 %all-to-all-start = ((f32[16,16,128]{2,1,0:T(8,128)}), f32[16,16,128]{2,1,0:T(8,128)S(1)}, u32[]{:S(2)}, u32[]{:S(2)}) async-start(f32[16,16,128]{2,1,0:T(8,128)} %get-tuple-element.25), calls=%async_computation | async-start | bytes 262144 | tf_op jit(solution)/shard_map/all_to_all | solution.py:359
  9.2 2.0 collective-permute-start
  11.3 3.4 %collective-permute-start.1 = (bf16[64,512]{1,0:T(8,128)(2,1)S(1)}, bf16[64,512]{1,0:T(8,128)(2,1)S(1)}, u32[]{:S(2)}, u32[]{:S(2)}) collective-permute-start(bf16[64,512]{1,0:T(8,128)(2,1)S(1)} %get-tuple-element.28), channel_id=1, source_target_pairs={{0,4},{2,6},{4,8},{6,10},{8,12},{10,14},{12,16},{14,18},{16,20},{1... | collective-permute-start | bytes 196616 | tf_op jit(solution)/shard_map/ppermute | solution.py:35
  14.6 3.4 %collective-permute-start.2 = (bf16[64,512]{1,0:T(8,128)(2,1)S(1)}, bf16[64,512]{1,0:T(8,128)(2,1)S(1)}, u32[]{:S(2)}, u32[]{:S(2)}) collective-permute-start(bf16[64,512]{1,0:T(8,128)(2,1)S(1)} %get-tuple-element.29), channel_id=1, source_target_pairs={{0,8},{2,10},{4,12},{6,14},{8,16},{10,18},{12,20},{14,22},{16,24},... | collective-permute-start | bytes 196616 | tf_op jit(solution)/shard_map/ppermute | solution.py:35
  18.0 2.2 collective-permute-start.3
  20.2 0.1 stack.34.where_ref
  20.3 0.0 collective-permute-done.refs_0_
  20.3 0.0 collective-permute-done.1.refs_1_
  20.3 1.0 collective-permute-done.2.refs_2_
  21.3 0.8 collective-permute-done.3.refs_3_
  22.1 0.0 all-to-all-done.news_ref
  22.1 2.5 shard_map.138
  24.6 1.6 collective-permute-start.4
  26.2 1.8 shard_map.137
  28.0 1.6 collective-permute-done.4.refs_1_
  29.6 1.3 shard_map.139.mapped_ref
  30.9 0.0 copy-done
  30.9 4.8 %shard_map.140 = (bf16[512,2048]{1,0:T(8,128)(2,1)}, bf16[256,2048]{1,0:T(8,128)(2,1)}) custom-call(s32[5]{0:T(128)S(1)} %stack.34.where_ref, bf16[256,512]{1,0:T(8,128)(2,1)S(1)} %shard_map.139.mapped_ref, bf16[512,2048]{1,0:T(8,128)(2,1)S(1)} %copy-done, f32[1,2048]{1,0:T(1,128)} %bitcast.34, f32[1,2048]{1,0:T(1,128)} %bitcast.36, ...), custom_call_target="tpu_custom_call" | custom-call | bytes 6832148 | tf_op jit(solution)/shard_map/pallas_call | solution.py:67
  35.7 6.8 %all-to-all-start.1 = ((bf16[16,32,2048]{2,1,0:T(8,128)(2,1)}), bf16[16,32,2048]{2,1,0:T(8,128)(2,1)}, u32[]{:S(2)}, u32[]{:S(2)}) async-start(bf16[16,32,2048]{2,1,0:T(8,128)(2,1)} %bitcast.30), calls=%async_computation.1 | async-start | bytes 4194304 | tf_op jit(solution)/shard_map/all_to_all | solution.py:397
  42.6 3.9 %collective-permute-start.8 = (bf16[256,2048]{1,0:T(8,128)(2,1)}, bf16[256,2048]{1,0:T(8,128)(2,1)S(1)}, u32[]{:S(2)}, u32[]{:S(2)}) collective-permute-start(bf16[256,2048]{1,0:T(8,128)(2,1)} %get-tuple-element.41), channel_id=1, source_target_pairs={{8,16},{16,8},{9,17},{17,9},{10,18},{18,10},{11,19},{19,11},{12,20... | collective-permute-start | bytes 3145736 | tf_op jit(solution)/shard_map/ppermute | solution.py:30
  46.5 1.5 collective-permute-start.6
  48.0 1.5 collective-permute-start.7
  49.5 0.0 collective-permute-start.5
  49.5 0.1 stack.36.where_ref
  49.6 1.9 shard_map.144
  51.5 0.0 collective-permute-done.6.refs_0_
  51.5 0.0 collective-permute-done.7.refs_1_
  51.5 52.6 %collective-permute-done.5.mapped_ref = bf16[256,512]{1,0:T(8,128)(2,1)} collective-permute-done((bf16[256,512]{1,0:T(8,128)(2,1)S(1)}, bf16[256,512]{1,0:T(8,128)(2,1)}, u32[]{:S(2)}, u32[]{:S(2)}) %collective-permute-start.5) | collective-permute-done | bytes 262176 | tf_op jit(solution)/shard_map/ppermute | solution.py:30
  104.1 0.0 collective-permute-done.8.refs_2_
  104.1 4.8 %shard_map.145 = bf16[512,2048]{1,0:T(8,128)(2,1)} custom-call(s32[5]{0:T(128)S(1)} %stack.36.where_ref, bf16[256,512]{1,0:T(8,128)(2,1)} %collective-permute-done.5.mapped_ref, bf16[512,2048]{1,0:T(8,128)(2,1)S(1)} %copy-done, f32[1,2048]{1,0:T(1,128)} %bitcast.35, f32[1,2048]{1,0:T(1,128)} %bitcast.37, bf16[512,256]{1,0:T(8,128)(2,1)S(1)} %get-tuple-element.38.pick_ref, ...), custom_call_target="tpu_custom_call" | custom-call | bytes 6832148 | tf_op jit(solution)/shard_map/pallas_call | solution.py:67
  108.8 0.0 all-to-all-done.1
  108.9 5.3 %all-to-all-start.4 = ((bf16[16,32,2048]{2,1,0:T(8,128)(2,1)}), bf16[16,32,2048]{2,1,0:T(8,128)(2,1)S(1)}, u32[]{:S(2)}, u32[]{:S(2)}) async-start(bf16[16,32,2048]{2,1,0:T(8,128)(2,1)} %bitcast.28), calls=%async_computation.4 | async-start | bytes 4194304 | tf_op jit(solution)/shard_map/all_to_all | solution.py:397
  114.2 13.4 %shard_map.141 = (bf16[512,1024]{1,0:T(8,128)(2,1)}, bf16[512,1024]{1,0:T(8,128)(2,1)}, bf16[512,1024]{1,0:T(8,128)(2,1)}) custom-call(bf16[512,2048]{1,0:T(8,128)(2,1)} %bitcast.11.x_ref, bf16[1,2048,1024]{2,1,0:T(8,128)(2,1)} %gate_ref.3, bf16[1,2048,1024]{2,1,0:T(8,128)(2,1)} %up_ref.3, bf16[1,1024,2048]{2,1,0:T(8,128)(2,1)} %down_ref.5), custom_call_target="tpu_custom_call" | custom-call | flops 6442450944 | bytes 16777216 | tf_op jit(solution)/shard_map/pallas_call | solution.py:260
  127.6 11.6 %all-to-all-done.4 = bf16[16,32,2048]{2,1,0:T(8,128)(2,1)S(1)} async-done(((bf16[16,32,2048]{2,1,0:T(8,128)(2,1)}), bf16[16,32,2048]{2,1,0:T(8,128)(2,1)S(1)}, u32[]{:S(2)}, u32[]{:S(2)}) %all-to-all-start.4) | async-done | bytes 2097184 | tf_op jit(solution)/shard_map/all_to_all | solution.py:397
  139.1 7.3 %all-to-all-start.3 = ((bf16[16,32,1024]{2,1,0:T(8,128)(2,1)}), bf16[16,32,1024]{2,1,0:T(8,128)(2,1)S(1)}, u32[]{:S(2)}, u32[]{:S(2)}) async-start(bf16[16,32,1024]{2,1,0:T(8,128)(2,1)} %bitcast.32), calls=%async_computation.3 | async-start | bytes 2097152 | tf_op jit(solution)/shard_map/all_to_all | solution.py:397
  146.5 10.3 %shard_map.146 = (bf16[512,1024]{1,0:T(8,128)(2,1)}, bf16[512,1024]{1,0:T(8,128)(2,1)}) custom-call(bf16[512,2048]{1,0:T(8,128)(2,1)S(1)} %bitcast.27, bf16[1,2048,1024]{2,1,0:T(8,128)(2,1)} %gate_ref.3, bf16[1,2048,1024]{2,1,0:T(8,128)(2,1)} %up_ref.3, bf16[1,1024,2048]{2,1,0:T(8,128)(2,1)} %down_ref.5), custom_call_target="tpu_custom_call" | custom-call | flops 5368709120 | bytes 14680064 | tf_op jit(solution)/shard_map/pallas_call | solution.py:260
  156.8 0.0 copy-start.4
  156.8 3.5 %all-to-all-done.3 = bf16[16,32,1024]{2,1,0:T(8,128)(2,1)S(1)} async-done(((bf16[16,32,1024]{2,1,0:T(8,128)(2,1)}), bf16[16,32,1024]{2,1,0:T(8,128)(2,1)S(1)}, u32[]{:S(2)}, u32[]{:S(2)}) %all-to-all-start.3) | async-done | bytes 1048608 | tf_op jit(solution)/shard_map/all_to_all | solution.py:397
  160.3 4.6 %all-to-all-start.5 = ((bf16[16,32,1024]{2,1,0:T(8,128)(2,1)}), bf16[16,32,1024]{2,1,0:T(8,128)(2,1)S(1)}, u32[]{:S(2)}, u32[]{:S(2)}) async-start(bf16[16,32,1024]{2,1,0:T(8,128)(2,1)} %bitcast.33), calls=%async_computation.5 | async-start | bytes 2097152 | tf_op jit(solution)/shard_map/all_to_all | solution.py:397
  164.9 0.0 copy-done.4
  164.9 3.8 %shard_map.148 = bf16[512,1024]{1,0:T(8,128)(2,1)} custom-call(bf16[512,1024]{1,0:T(8,128)(2,1)S(1)} %copy-done.4, bf16[1,1024,2048]{2,1,0:T(8,128)(2,1)} %down_ref.5), custom_call_target="tpu_custom_call" | custom-call | flops 1073741824 | bytes 4194304 | tf_op jit(solution)/shard_map/pallas_call | solution.py:291
  168.7 10.4 %all-to-all-done.5 = bf16[16,32,1024]{2,1,0:T(8,128)(2,1)S(1)} async-done(((bf16[16,32,1024]{2,1,0:T(8,128)(2,1)}), bf16[16,32,1024]{2,1,0:T(8,128)(2,1)S(1)}, u32[]{:S(2)}, u32[]{:S(2)}) %all-to-all-start.5) | async-done | bytes 1048608 | tf_op jit(solution)/shard_map/all_to_all | solution.py:397
  179.1 18.3 %all_to_all.35 = bf16[16,32,1024]{2,1,0:T(8,128)(2,1)S(1)} all-to-all(bf16[16,32,1024]{2,1,0:T(8,128)(2,1)} %bitcast.29), channel_id=1, replica_groups=mesh['zh'=2,'zl'=2,'yc'=4,'tp'=2] {'zl','yc','tp'}, dimensions={0} | all-to-all | bytes 2097152 | tf_op jit(solution)/shard_map/all_to_all | solution.py:397
  197.4 4.8 %all-to-all-start.2 = ((bf16[16,32,1024]{2,1,0:T(8,128)(2,1)}), bf16[16,32,1024]{2,1,0:T(8,128)(2,1)}, u32[]{:S(2)}, u32[]{:S(2)}) async-start(bf16[16,32,1024]{2,1,0:T(8,128)(2,1)} %bitcast.31), calls=%async_computation.2 | async-start | bytes 2097152 | tf_op jit(solution)/shard_map/all_to_all | solution.py:397
  202.2 0.0 copy-start.2
  202.2 0.0 copy-start.3
  202.2 1.0 copy-done.3
  203.2 1.2 shard_map.147
  204.4 0.5 collective-permute-start.9
  204.9 1.2 shard_map.149
  206.2 1.5 collective-permute-start.10
  207.7 0.0 copy-done.2
  207.7 0.0 copy-start.1
  207.7 0.4 shard_map.143.own_1
  208.1 7.5 %all-to-all-done.2 = bf16[16,32,1024]{2,1,0:T(8,128)(2,1)} async-done(((bf16[16,32,1024]{2,1,0:T(8,128)(2,1)}), bf16[16,32,1024]{2,1,0:T(8,128)(2,1)}, u32[]{:S(2)}, u32[]{:S(2)}) %all-to-all-start.2) | async-done | bytes 1048608 | tf_op jit(solution)/shard_map/all_to_all | solution.py:397
  215.6 1.7 shard_map.142.own_0
  217.3 24.7 %collective-permute-done.9.other_0 = bf16[256,1024]{1,0:T(8,128)(2,1)} collective-permute-done((bf16[256,1024]{1,0:T(8,128)(2,1)}, bf16[256,1024]{1,0:T(8,128)(2,1)}, u32[]{:S(2)}, u32[]{:S(2)}) %collective-permute-start.9) | collective-permute-done | bytes 524320 | tf_op jit(solution)/shard_map/ppermute | solution.py:30
  242.0 10.4 %collective-permute-done.10.other_1 = bf16[256,1024]{1,0:T(8,128)(2,1)} collective-permute-done((bf16[256,1024]{1,0:T(8,128)(2,1)}, bf16[256,1024]{1,0:T(8,128)(2,1)}, u32[]{:S(2)}, u32[]{:S(2)}) %collective-permute-start.10) | collective-permute-done | bytes 524320 | tf_op jit(solution)/shard_map/ppermute | solution.py:30
  252.4 0.0 copy-done.1
  252.4 3.1 %shard_map.150 = bf16[256,2048]{1,0:T(8,128)(2,1)} custom-call(f32[256,1024]{1,0:T(8,128)S(1)} %shard_map.142.own_0, f32[256,1024]{1,0:T(8,128)S(1)} %shard_map.143.own_1, bf16[256,1024]{1,0:T(8,128)(2,1)} %collective-permute-done.9.other_0, bf16[256,1024]{1,0:T(8,128)(2,1)} %collective-permute-done.10.other_1, bf16[256,2048]{1,0:T(8,128)(2,1)S(1)} %copy-done.1, ...), custom_call_target="tpu_custom_call" | custom-call | bytes 5251072 | tf_op jit(solution)/shard_map/pallas_call | solution.py:67
Async XLA Ops:
  0.0 30.9 %copy-start = (bf16[512,2048]{1,0:T(8,128)(2,1)S(1)}, bf16[512,2048]{1,0:T(8,128)(2,1)}, u32[]{:S(2)}) copy-start(bf16[512,2048]{1,0:T(8,128)(2,1)} %w_ref.3) | copy-start | bytes 6291460
  2.9 19.2 %all-to-all-start = ((f32[16,16,128]{2,1,0:T(8,128)}), f32[16,16,128]{2,1,0:T(8,128)S(1)}, u32[]{:S(2)}, u32[]{:S(2)}) async-start(f32[16,16,128]{2,1,0:T(8,128)} %get-tuple-element.25), calls=%async_computation | async-start | bytes 262144 | tf_op jit(solution)/shard_map/all_to_all | solution.py:359
  9.2 11.1 %collective-permute-start = (bf16[64,512]{1,0:T(8,128)(2,1)S(1)}, bf16[64,512]{1,0:T(8,128)(2,1)S(1)}, u32[]{:S(2)}, u32[]{:S(2)}) collective-permute-start(bf16[64,512]{1,0:T(8,128)(2,1)S(1)} %get-tuple-element.27), channel_id=1, source_target_pairs={{0,2},{2,4},{4,6},{6,8},{8,10},{10,12},{12,14},{14,16},{16,18},{18... | collective-permute-start | bytes 196616 | tf_op jit(solution)/shard_map/ppermute | solution.py:35
  11.3 9.1 %collective-permute-start.1 = (bf16[64,512]{1,0:T(8,128)(2,1)S(1)}, bf16[64,512]{1,0:T(8,128)(2,1)S(1)}, u32[]{:S(2)}, u32[]{:S(2)}) collective-permute-start(bf16[64,512]{1,0:T(8,128)(2,1)S(1)} %get-tuple-element.28), channel_id=1, source_target_pairs={{0,4},{2,6},{4,8},{6,10},{8,12},{10,14},{12,16},{14,18},{16,20},{1... | collective-permute-start | bytes 196616 | tf_op jit(solution)/shard_map/ppermute | solution.py:35
  14.6 6.6 %collective-permute-start.2 = (bf16[64,512]{1,0:T(8,128)(2,1)S(1)}, bf16[64,512]{1,0:T(8,128)(2,1)S(1)}, u32[]{:S(2)}, u32[]{:S(2)}) collective-permute-start(bf16[64,512]{1,0:T(8,128)(2,1)S(1)} %get-tuple-element.29), channel_id=1, source_target_pairs={{0,8},{2,10},{4,12},{6,14},{8,16},{10,18},{12,20},{14,22},{16,24},... | collective-permute-start | bytes 196616 | tf_op jit(solution)/shard_map/ppermute | solution.py:35
  18.0 4.1 %collective-permute-start.3 = (bf16[64,512]{1,0:T(8,128)(2,1)S(1)}, bf16[64,512]{1,0:T(8,128)(2,1)S(1)}, u32[]{:S(2)}, u32[]{:S(2)}) collective-permute-start(bf16[64,512]{1,0:T(8,128)(2,1)S(1)} %get-tuple-element.30), channel_id=1, source_target_pairs={{0,16},{2,18},{4,20},{6,22},{8,24},{10,26},{12,28},{14,30},{1,17},... | collective-permute-start | bytes 196616 | tf_op jit(solution)/shard_map/ppermute | solution.py:35
  24.6 5.0 %collective-permute-start.4 = (bf16[4,64,256]{2,1,0:T(8,128)(2,1)S(1)}, bf16[4,64,256]{2,1,0:T(8,128)(2,1)S(1)}, u32[]{:S(2)}, u32[]{:S(2)}) collective-permute-start(bf16[4,64,256]{2,1,0:T(8,128)(2,1)S(1)} %get-tuple-element.32), channel_id=1, source_target_pairs={{0,1},{1,0},{2,3},{3,2},{4,5},{5,4},{6,7},{7,6},{8,9},{9,8},{10,11... | collective-permute-start | bytes 393224 | tf_op jit(solution)/shard_map/ppermute | solution.py:378
  35.7 73.1 %all-to-all-start.1 = ((bf16[16,32,2048]{2,1,0:T(8,128)(2,1)}), bf16[16,32,2048]{2,1,0:T(8,128)(2,1)}, u32[]{:S(2)}, u32[]{:S(2)}) async-start(bf16[16,32,2048]{2,1,0:T(8,128)(2,1)} %bitcast.30), calls=%async_computation.1 | async-start | bytes 4194304 | tf_op jit(solution)/shard_map/all_to_all | solution.py:397
  42.6 61.5 %collective-permute-start.8 = (bf16[256,2048]{1,0:T(8,128)(2,1)}, bf16[256,2048]{1,0:T(8,128)(2,1)S(1)}, u32[]{:S(2)}, u32[]{:S(2)}) collective-permute-start(bf16[256,2048]{1,0:T(8,128)(2,1)} %get-tuple-element.41), channel_id=1, source_target_pairs={{8,16},{16,8},{9,17},{17,9},{10,18},{18,10},{11,19},{19,11},{12,20... | collective-permute-start | bytes 3145736 | tf_op jit(solution)/shard_map/ppermute | solution.py:30
  46.5 5.0 %collective-permute-start.6 = (bf16[128,2048]{1,0:T(8,128)(2,1)}, bf16[128,2048]{1,0:T(8,128)(2,1)}, u32[]{:S(2)}, u32[]{:S(2)}) collective-permute-start(bf16[128,2048]{1,0:T(8,128)(2,1)} %get-tuple-element.39), channel_id=1, source_target_pairs={{0,24},{24,0},{1,25},{25,1},{2,26},{26,2},{3,27},{27,3},{4,28},{28... | collective-permute-start | bytes 1572872 | tf_op jit(solution)/shard_map/ppermute | solution.py:30
  48.0 3.5 %collective-permute-start.7 = (bf16[128,2048]{1,0:T(8,128)(2,1)}, bf16[128,2048]{1,0:T(8,128)(2,1)}, u32[]{:S(2)}, u32[]{:S(2)}) collective-permute-start(bf16[128,2048]{1,0:T(8,128)(2,1)} %get-tuple-element.40), channel_id=1, source_target_pairs={{0,24},{24,0},{1,25},{25,1},{2,26},{26,2},{3,27},{27,3},{4,28},{28... | collective-permute-start | bytes 1572872 | tf_op jit(solution)/shard_map/ppermute | solution.py:30
  49.5 54.5 %collective-permute-start.5 = (bf16[256,512]{1,0:T(8,128)(2,1)S(1)}, bf16[256,512]{1,0:T(8,128)(2,1)}, u32[]{:S(2)}, u32[]{:S(2)}) collective-permute-start(bf16[256,512]{1,0:T(8,128)(2,1)S(1)} %shard_map.139.mapped_ref), channel_id=1, source_target_pairs={{0,24},{8,16},{16,8},{24,0},{1,25},{9,17},{17,9},{25,1},{2,26},{10... | collective-permute-start | bytes 786440 | tf_op jit(solution)/shard_map/ppermute | solution.py:30
  108.9 30.3 %all-to-all-start.4 = ((bf16[16,32,2048]{2,1,0:T(8,128)(2,1)}), bf16[16,32,2048]{2,1,0:T(8,128)(2,1)S(1)}, u32[]{:S(2)}, u32[]{:S(2)}) async-start(bf16[16,32,2048]{2,1,0:T(8,128)(2,1)} %bitcast.28), calls=%async_computation.4 | async-start | bytes 4194304 | tf_op jit(solution)/shard_map/all_to_all | solution.py:397
  139.1 21.1 %all-to-all-start.3 = ((bf16[16,32,1024]{2,1,0:T(8,128)(2,1)}), bf16[16,32,1024]{2,1,0:T(8,128)(2,1)S(1)}, u32[]{:S(2)}, u32[]{:S(2)}) async-start(bf16[16,32,1024]{2,1,0:T(8,128)(2,1)} %bitcast.32), calls=%async_computation.3 | async-start | bytes 2097152 | tf_op jit(solution)/shard_map/all_to_all | solution.py:397
  156.8 8.1 %copy-start.4 = (bf16[512,1024]{1,0:T(8,128)(2,1)S(1)}, bf16[512,1024]{1,0:T(8,128)(2,1)}, u32[]{:S(2)}) copy-start(bf16[512,1024]{1,0:T(8,128)(2,1)} %get-tuple-element.43.hidden_ref) | copy-start | bytes 3145732
  160.3 18.8 %all-to-all-start.5 = ((bf16[16,32,1024]{2,1,0:T(8,128)(2,1)}), bf16[16,32,1024]{2,1,0:T(8,128)(2,1)S(1)}, u32[]{:S(2)}, u32[]{:S(2)}) async-start(bf16[16,32,1024]{2,1,0:T(8,128)(2,1)} %bitcast.33), calls=%async_computation.5 | async-start | bytes 2097152 | tf_op jit(solution)/shard_map/all_to_all | solution.py:397
  197.4 18.2 %all-to-all-start.2 = ((bf16[16,32,1024]{2,1,0:T(8,128)(2,1)}), bf16[16,32,1024]{2,1,0:T(8,128)(2,1)}, u32[]{:S(2)}, u32[]{:S(2)}) async-start(bf16[16,32,1024]{2,1,0:T(8,128)(2,1)} %bitcast.31), calls=%async_computation.2 | async-start | bytes 2097152 | tf_op jit(solution)/shard_map/all_to_all | solution.py:397
  202.2 5.5 %copy-start.2 = (bf16[256,512]{1,0:T(8,128)(2,1)S(1)}, bf16[256,512]{1,0:T(8,128)(2,1)}, u32[]{:S(2)}) copy-start(bf16[256,512]{1,0:T(8,128)(2,1)} %get-tuple-element.26.weight_ref) | copy-start | bytes 786436
  202.2 1.0 copy-start.3
  204.4 37.6 %collective-permute-start.9 = (bf16[256,1024]{1,0:T(8,128)(2,1)}, bf16[256,1024]{1,0:T(8,128)(2,1)}, u32[]{:S(2)}, u32[]{:S(2)}) collective-permute-start(bf16[256,1024]{1,0:T(8,128)(2,1)} %shard_map.147), channel_id=1, source_target_pairs={{0,24},{8,16},{16,8},{24,0},{1,25},{9,17},{17,9},{25,1},{2,26},{10... | collective-permute-start | bytes 1572872 | tf_op jit(solution)/shard_map/ppermute | solution.py:30
  206.2 46.2 %collective-permute-start.10 = (bf16[256,1024]{1,0:T(8,128)(2,1)}, bf16[256,1024]{1,0:T(8,128)(2,1)}, u32[]{:S(2)}, u32[]{:S(2)}) collective-permute-start(bf16[256,1024]{1,0:T(8,128)(2,1)} %shard_map.149), channel_id=1, source_target_pairs={{0,24},{8,16},{16,8},{24,0},{1,25},{9,17},{17,9},{25,1},{2,26},{10... | collective-permute-start | bytes 1572872 | tf_op jit(solution)/shard_map/ppermute | solution.py:30
  207.7 44.7 %copy-start.1 = (bf16[256,2048]{1,0:T(8,128)(2,1)S(1)}, bf16[256,2048]{1,0:T(8,128)(2,1)}, u32[]{:S(2)}) copy-start(bf16[256,2048]{1,0:T(8,128)(2,1)} %get-tuple-element.44.stream_ref) | copy-start | bytes 3145732

commit v3 on v2

--- a/solution.py
+++ b/solution.py
@@ -80,7 +80,6 @@
     part = piece_refs[0].shape[0]
     piece_refs[0][...] = res_ref[:part]
     piece_refs[1][...] = res_ref[part:]
-    piece_refs[2][...] = res_ref[...]
     blocks = news_ref.shape[0]
     docs = docs_ref[...]
     tail = docs == docs[:, length - 1 :]
@@ -339,11 +338,12 @@
     own_at = jnp.stack([mine, mine, first, column_at, edge])
     far_at = jnp.stack([mine, twin, first, column_at, edge])
     docs = in_hbm(doc_ids.reshape(1, length))
+    residual_in = residual
     pool_input, residual = in_hbm(pool_input), in_hbm(residual)
     skip = groups * channels // LANES + 2
     lines = skip + 4 * rows // LANES
     lines += -lines % 8
-    sizes = (rows // 2, rows // 2, rows)
+    sizes = (rows // 2, rows // 2)
     news, *own_blocks = call(
         head_kernel,
         [((blocks, lines, LANES), F32)]
@@ -355,7 +355,7 @@
         in_hbm(route_logits.T),
         residual,
     )
-    own_blocks, pieces = own_blocks[:groups], own_blocks[groups:]
+    own_blocks, pieces = own_blocks[:groups], [*own_blocks[groups:], residual_in]
     news = (lax.all_to_all(news, SP, 0, 0, tiled=True))
     far_blocks = []
     for g in range(groups):

time: 256 us -> 256 us (level)
  no operation moved by 1% of the time
where the time goes in v3:
time: 256 us; the launch traced here: 255 us
  waiting for transfers between devices  124 us (48%)
  starting transfers between devices  56.5 us (22%)
  Pallas kernels  54.7 us (21%)
  blocking collectives  18.3 us (7%)
    ppermute x6, waiting for transfers between devices, to_twin(): return lax.ppermute(x, ('zh', 'zl'), [(i, last - i) for i in used])  87.8 us
    all_to_all x5, waiting for transfers between devices, there(): return lax.all_to_all(x, HALF, 0, 0, tiled=True).reshape(-1, columns)  33.1 us
    all_to_all x5, starting transfers between devices, there(): return lax.all_to_all(x, HALF, 0, 0, tiled=True).reshape(-1, columns)  28.8 us
    pallas_call x12, Pallas kernels, call(): pl.pallas_call(kernel, out_shape=shapes, in_specs=specs, out_specs=[VM] *...  27.3 us
    pallas_call x2, Pallas kernels, expert_rows(): pl.pallas_call(functools.partial(expert_kernel, tiles), grid=(tiles + par...  23.6 us
    all_to_all x1, blocking collectives, there(): return lax.all_to_all(x, HALF, 0, 0, tiled=True).reshape(-1, columns)  18.3 us
    ppermute x4, starting transfers between devices, passed_along(): return lax.ppermute(x, SP, [(i, i + by) for i in range(devices - by)])  10.9 us
    ppermute x6, starting transfers between devices, to_twin(): return lax.ppermute(x, ('zh', 'zl'), [(i, last - i) for i in used])  8.9 us
  transfers between devices with their start and end apart: 17, of which 10 were waited for; matrix products, arithmetic and copies ran while one was open for 0% of the time, Pallas kernels for 16%

profile of v3, /device:TPU:8, one launch (start us, length us, event | category | flops | bytes accessed | tf_op | source)
XLA Modules:
  0.0 255.2 jit_solution(7343990332767119853)
XLA Ops:
  0.0 0.0 copy-start
  0.0 2.6 %shard_map.136 = (f32[16,16,128]{2,1,0:T(8,128)}, bf16[64,512]{1,0:T(8,128)(2,1)S(1)}, bf16[64,512]{1,0:T(8,128)(2,1)S(1)}, bf16[64,512]{1,0:T(8,128)(2,1)S(1)},...) custom-call(bf16[4,64,512]{2,1,0:T(8,128)(2,1)} %x_ref.3, s32[1,512]{1,0:T(1,128)} %bitcast.39, ...), custom_call_target="tpu_custom_call" | custom-call | bytes 2758656 | tf_op jit(solution)/shard_map/pallas_call | solution.py:67
  2.6 6.3 %all-to-all-start = ((f32[16,16,128]{2,1,0:T(8,128)}), f32[16,16,128]{2,1,0:T(8,128)S(1)}, u32[]{:S(2)}, u32[]{:S(2)}) async-start(f32[16,16,128]{2,1,0:T(8,128)} %get-tuple-element.24), calls=%async_computation | async-start | bytes 262144 | tf_op jit(solution)/shard_map/all_to_all | solution.py:359
  8.9 2.0 collective-permute-start
  11.0 3.4 %collective-permute-start.1 = (bf16[64,512]{1,0:T(8,128)(2,1)S(1)}, bf16[64,512]{1,0:T(8,128)(2,1)S(1)}, u32[]{:S(2)}, u32[]{:S(2)}) collective-permute-start(bf16[64,512]{1,0:T(8,128)(2,1)S(1)} %get-tuple-element.27), channel_id=1, source_target_pairs={{0,4},{2,6},{4,8},{6,10},{8,12},{10,14},{12,16},{14,18},{16,20},{1... | collective-permute-start | bytes 196616 | tf_op jit(solution)/shard_map/ppermute | solution.py:35
  14.3 3.4 %collective-permute-start.2 = (bf16[64,512]{1,0:T(8,128)(2,1)S(1)}, bf16[64,512]{1,0:T(8,128)(2,1)S(1)}, u32[]{:S(2)}, u32[]{:S(2)}) collective-permute-start(bf16[64,512]{1,0:T(8,128)(2,1)S(1)} %get-tuple-element.28), channel_id=1, source_target_pairs={{0,8},{2,10},{4,12},{6,14},{8,16},{10,18},{12,20},{14,22},{16,24},... | collective-permute-start | bytes 196616 | tf_op jit(solution)/shard_map/ppermute | solution.py:35
  17.7 2.2 collective-permute-start.3
  19.9 0.1 stack.34.where_ref
  20.0 0.0 collective-permute-done.refs_0_
  20.0 0.0 collective-permute-done.1.refs_1_
  20.0 1.0 collective-permute-done.2.refs_2_
  21.0 0.8 collective-permute-done.3.refs_3_
  21.8 0.0 all-to-all-done.news_ref
  21.8 2.5 shard_map.138
  24.3 1.6 collective-permute-start.4
  25.9 1.8 shard_map.137
  27.7 1.7 collective-permute-done.4.refs_1_
  29.3 1.3 shard_map.139.mapped_ref
  30.6 0.0 copy-done
  30.6 4.8 %shard_map.140 = (bf16[512,2048]{1,0:T(8,128)(2,1)}, bf16[256,2048]{1,0:T(8,128)(2,1)}) custom-call(s32[5]{0:T(128)S(1)} %stack.34.where_ref, bf16[256,512]{1,0:T(8,128)(2,1)S(1)} %shard_map.139.mapped_ref, bf16[512,2048]{1,0:T(8,128)(2,1)S(1)} %copy-done, f32[1,2048]{1,0:T(1,128)} %bitcast.34, f32[1,2048]{1,0:T(1,128)} %bitcast.36, ...), custom_call_target="tpu_custom_call" | custom-call | bytes 6832148 | tf_op jit(solution)/shard_map/pallas_call | solution.py:67
  35.4 6.9 %all-to-all-start.1 = ((bf16[16,32,2048]{2,1,0:T(8,128)(2,1)}), bf16[16,32,2048]{2,1,0:T(8,128)(2,1)}, u32[]{:S(2)}, u32[]{:S(2)}) async-start(bf16[16,32,2048]{2,1,0:T(8,128)(2,1)} %bitcast.30), calls=%async_computation.1 | async-start | bytes 4194304 | tf_op jit(solution)/shard_map/all_to_all | solution.py:397
  42.3 3.9 %collective-permute-start.8 = (bf16[256,2048]{1,0:T(8,128)(2,1)}, bf16[256,2048]{1,0:T(8,128)(2,1)S(1)}, u32[]{:S(2)}, u32[]{:S(2)}) collective-permute-start(bf16[256,2048]{1,0:T(8,128)(2,1)} %refs_0_.1), channel_id=1, source_target_pairs={{8,16},{16,8},{9,17},{17,9},{10,18},{18,10},{11,19},{19,11},{12,20... | collective-permute-start | bytes 3145736 | tf_op jit(solution)/shard_map/ppermute | solution.py:30
  46.2 1.5 collective-permute-start.6
  47.7 1.4 collective-permute-start.7
  49.2 0.0 collective-permute-start.5
  49.2 0.1 stack.36.where_ref
  49.3 1.9 shard_map.144
  51.1 0.0 collective-permute-done.6.refs_0_
  51.1 0.0 collective-permute-done.7.refs_1_
  51.1 52.7 %collective-permute-done.5.mapped_ref = bf16[256,512]{1,0:T(8,128)(2,1)} collective-permute-done((bf16[256,512]{1,0:T(8,128)(2,1)S(1)}, bf16[256,512]{1,0:T(8,128)(2,1)}, u32[]{:S(2)}, u32[]{:S(2)}) %collective-permute-start.5) | collective-permute-done | bytes 262176 | tf_op jit(solution)/shard_map/ppermute | solution.py:30
  103.8 0.0 collective-permute-done.8.refs_2_
  103.8 4.8 %shard_map.145 = bf16[512,2048]{1,0:T(8,128)(2,1)} custom-call(s32[5]{0:T(128)S(1)} %stack.36.where_ref, bf16[256,512]{1,0:T(8,128)(2,1)} %collective-permute-done.5.mapped_ref, bf16[512,2048]{1,0:T(8,128)(2,1)S(1)} %copy-done, f32[1,2048]{1,0:T(1,128)} %bitcast.35, f32[1,2048]{1,0:T(1,128)} %bitcast.37, bf16[512,256]{1,0:T(8,128)(2,1)S(1)} %get-tuple-element.37.pick_ref, ...), custom_call_target="tpu_custom_call" | custom-call | bytes 6832148 | tf_op jit(solution)/shard_map/pallas_call | solution.py:67
  108.6 0.0 all-to-all-done.1
  108.6 5.3 %all-to-all-start.4 = ((bf16[16,32,2048]{2,1,0:T(8,128)(2,1)}), bf16[16,32,2048]{2,1,0:T(8,128)(2,1)S(1)}, u32[]{:S(2)}, u32[]{:S(2)}) async-start(bf16[16,32,2048]{2,1,0:T(8,128)(2,1)} %bitcast.28), calls=%async_computation.4 | async-start | bytes 4194304 | tf_op jit(solution)/shard_map/all_to_all | solution.py:397
  113.9 13.3 %shard_map.141 = (bf16[512,1024]{1,0:T(8,128)(2,1)}, bf16[512,1024]{1,0:T(8,128)(2,1)}, bf16[512,1024]{1,0:T(8,128)(2,1)}) custom-call(bf16[512,2048]{1,0:T(8,128)(2,1)} %bitcast.11.x_ref, bf16[1,2048,1024]{2,1,0:T(8,128)(2,1)} %gate_ref.3, bf16[1,2048,1024]{2,1,0:T(8,128)(2,1)} %up_ref.3, bf16[1,1024,2048]{2,1,0:T(8,128)(2,1)} %down_ref.5), custom_call_target="tpu_custom_call" | custom-call | flops 6442450944 | bytes 16777216 | tf_op jit(solution)/shard_map/pallas_call | solution.py:259
  127.2 11.6 %all-to-all-done.4 = bf16[16,32,2048]{2,1,0:T(8,128)(2,1)S(1)} async-done(((bf16[16,32,2048]{2,1,0:T(8,128)(2,1)}), bf16[16,32,2048]{2,1,0:T(8,128)(2,1)S(1)}, u32[]{:S(2)}, u32[]{:S(2)}) %all-to-all-start.4) | async-done | bytes 2097184 | tf_op jit(solution)/shard_map/all_to_all | solution.py:397
  138.9 7.3 %all-to-all-start.3 = ((bf16[16,32,1024]{2,1,0:T(8,128)(2,1)}), bf16[16,32,1024]{2,1,0:T(8,128)(2,1)S(1)}, u32[]{:S(2)}, u32[]{:S(2)}) async-start(bf16[16,32,1024]{2,1,0:T(8,128)(2,1)} %bitcast.32), calls=%async_computation.3 | async-start | bytes 2097152 | tf_op jit(solution)/shard_map/all_to_all | solution.py:397
  146.2 10.3 %shard_map.146 = (bf16[512,1024]{1,0:T(8,128)(2,1)}, bf16[512,1024]{1,0:T(8,128)(2,1)}) custom-call(bf16[512,2048]{1,0:T(8,128)(2,1)S(1)} %bitcast.27, bf16[1,2048,1024]{2,1,0:T(8,128)(2,1)} %gate_ref.3, bf16[1,2048,1024]{2,1,0:T(8,128)(2,1)} %up_ref.3, bf16[1,1024,2048]{2,1,0:T(8,128)(2,1)} %down_ref.5), custom_call_target="tpu_custom_call" | custom-call | flops 5368709120 | bytes 14680064 | tf_op jit(solution)/shard_map/pallas_call | solution.py:259
  156.5 0.0 copy-start.4
  156.5 3.5 %all-to-all-done.3 = bf16[16,32,1024]{2,1,0:T(8,128)(2,1)S(1)} async-done(((bf16[16,32,1024]{2,1,0:T(8,128)(2,1)}), bf16[16,32,1024]{2,1,0:T(8,128)(2,1)S(1)}, u32[]{:S(2)}, u32[]{:S(2)}) %all-to-all-start.3) | async-done | bytes 1048608 | tf_op jit(solution)/shard_map/all_to_all | solution.py:397
  160.0 4.6 %all-to-all-start.5 = ((bf16[16,32,1024]{2,1,0:T(8,128)(2,1)}), bf16[16,32,1024]{2,1,0:T(8,128)(2,1)S(1)}, u32[]{:S(2)}, u32[]{:S(2)}) async-start(bf16[16,32,1024]{2,1,0:T(8,128)(2,1)} %bitcast.33), calls=%async_computation.5 | async-start | bytes 2097152 | tf_op jit(solution)/shard_map/all_to_all | solution.py:397
  164.6 0.0 copy-done.4
  164.6 3.8 %shard_map.148 = bf16[512,1024]{1,0:T(8,128)(2,1)} custom-call(bf16[512,1024]{1,0:T(8,128)(2,1)S(1)} %copy-done.4, bf16[1,1024,2048]{2,1,0:T(8,128)(2,1)} %down_ref.5), custom_call_target="tpu_custom_call" | custom-call | flops 1073741824 | bytes 4194304 | tf_op jit(solution)/shard_map/pallas_call | solution.py:290
  168.4 10.4 %all-to-all-done.5 = bf16[16,32,1024]{2,1,0:T(8,128)(2,1)S(1)} async-done(((bf16[16,32,1024]{2,1,0:T(8,128)(2,1)}), bf16[16,32,1024]{2,1,0:T(8,128)(2,1)S(1)}, u32[]{:S(2)}, u32[]{:S(2)}) %all-to-all-start.5) | async-done | bytes 1048608 | tf_op jit(solution)/shard_map/all_to_all | solution.py:397
  178.8 18.3 %all_to_all.35 = bf16[16,32,1024]{2,1,0:T(8,128)(2,1)S(1)} all-to-all(bf16[16,32,1024]{2,1,0:T(8,128)(2,1)} %bitcast.29), channel_id=1, replica_groups=mesh['zh'=2,'zl'=2,'yc'=4,'tp'=2] {'zl','yc','tp'}, dimensions={0} | all-to-all | bytes 2097152 | tf_op jit(solution)/shard_map/all_to_all | solution.py:397
  197.1 4.8 %all-to-all-start.2 = ((bf16[16,32,1024]{2,1,0:T(8,128)(2,1)}), bf16[16,32,1024]{2,1,0:T(8,128)(2,1)}, u32[]{:S(2)}, u32[]{:S(2)}) async-start(bf16[16,32,1024]{2,1,0:T(8,128)(2,1)} %bitcast.31), calls=%async_computation.2 | async-start | bytes 2097152 | tf_op jit(solution)/shard_map/all_to_all | solution.py:397
  201.9 0.0 copy-start.2
  201.9 0.0 copy-start.3
  201.9 1.0 copy-done.3
  202.9 1.2 shard_map.147
  204.1 0.5 collective-permute-start.9
  204.6 1.2 shard_map.149
  205.9 1.5 collective-permute-start.10
  207.4 0.0 copy-done.2
  207.4 0.0 copy-start.1
  207.4 0.4 shard_map.143.own_1
  207.8 7.5 %all-to-all-done.2 = bf16[16,32,1024]{2,1,0:T(8,128)(2,1)} async-done(((bf16[16,32,1024]{2,1,0:T(8,128)(2,1)}), bf16[16,32,1024]{2,1,0:T(8,128)(2,1)}, u32[]{:S(2)}, u32[]{:S(2)}) %all-to-all-start.2) | async-done | bytes 1048608 | tf_op jit(solution)/shard_map/all_to_all | solution.py:397
  215.3 1.7 shard_map.142.own_0
  217.0 24.7 %collective-permute-done.9.other_0 = bf16[256,1024]{1,0:T(8,128)(2,1)} collective-permute-done((bf16[256,1024]{1,0:T(8,128)(2,1)}, bf16[256,1024]{1,0:T(8,128)(2,1)}, u32[]{:S(2)}, u32[]{:S(2)}) %collective-permute-start.9) | collective-permute-done | bytes 524320 | tf_op jit(solution)/shard_map/ppermute | solution.py:30
  241.7 10.4 %collective-permute-done.10.other_1 = bf16[256,1024]{1,0:T(8,128)(2,1)} collective-permute-done((bf16[256,1024]{1,0:T(8,128)(2,1)}, bf16[256,1024]{1,0:T(8,128)(2,1)}, u32[]{:S(2)}, u32[]{:S(2)}) %collective-permute-start.10) | collective-permute-done | bytes 524320 | tf_op jit(solution)/shard_map/ppermute | solution.py:30
  252.1 0.0 copy-done.1
  252.1 3.1 %shard_map.150 = bf16[256,2048]{1,0:T(8,128)(2,1)} custom-call(f32[256,1024]{1,0:T(8,128)S(1)} %shard_map.142.own_0, f32[256,1024]{1,0:T(8,128)S(1)} %shard_map.143.own_1, bf16[256,1024]{1,0:T(8,128)(2,1)} %collective-permute-done.9.other_0, bf16[256,1024]{1,0:T(8,128)(2,1)} %collective-permute-done.10.other_1, bf16[256,2048]{1,0:T(8,128)(2,1)S(1)} %copy-done.1, ...), custom_call_target="tpu_custom_call" | custom-call | bytes 5251072 | tf_op jit(solution)/shard_map/pallas_call | solution.py:67
Async XLA Ops:
  0.0 30.6 %copy-start = (bf16[512,2048]{1,0:T(8,128)(2,1)S(1)}, bf16[512,2048]{1,0:T(8,128)(2,1)}, u32[]{:S(2)}) copy-start(bf16[512,2048]{1,0:T(8,128)(2,1)} %w_ref.3) | copy-start | bytes 6291460
  2.6 19.2 %all-to-all-start = ((f32[16,16,128]{2,1,0:T(8,128)}), f32[16,16,128]{2,1,0:T(8,128)S(1)}, u32[]{:S(2)}, u32[]{:S(2)}) async-start(f32[16,16,128]{2,1,0:T(8,128)} %get-tuple-element.24), calls=%async_computation | async-start | bytes 262144 | tf_op jit(solution)/shard_map/all_to_all | solution.py:359
  8.9 11.1 %collective-permute-start = (bf16[64,512]{1,0:T(8,128)(2,1)S(1)}, bf16[64,512]{1,0:T(8,128)(2,1)S(1)}, u32[]{:S(2)}, u32[]{:S(2)}) collective-permute-start(bf16[64,512]{1,0:T(8,128)(2,1)S(1)} %get-tuple-element.26), channel_id=1, source_target_pairs={{0,2},{2,4},{4,6},{6,8},{8,10},{10,12},{12,14},{14,16},{16,18},{18... | collective-permute-start | bytes 196616 | tf_op jit(solution)/shard_map/ppermute | solution.py:35
  11.0 9.1 %collective-permute-start.1 = (bf16[64,512]{1,0:T(8,128)(2,1)S(1)}, bf16[64,512]{1,0:T(8,128)(2,1)S(1)}, u32[]{:S(2)}, u32[]{:S(2)}) collective-permute-start(bf16[64,512]{1,0:T(8,128)(2,1)S(1)} %get-tuple-element.27), channel_id=1, source_target_pairs={{0,4},{2,6},{4,8},{6,10},{8,12},{10,14},{12,16},{14,18},{16,20},{1... | collective-permute-start | bytes 196616 | tf_op jit(solution)/shard_map/ppermute | solution.py:35
  14.3 6.6 %collective-permute-start.2 = (bf16[64,512]{1,0:T(8,128)(2,1)S(1)}, bf16[64,512]{1,0:T(8,128)(2,1)S(1)}, u32[]{:S(2)}, u32[]{:S(2)}) collective-permute-start(bf16[64,512]{1,0:T(8,128)(2,1)S(1)} %get-tuple-element.28), channel_id=1, source_target_pairs={{0,8},{2,10},{4,12},{6,14},{8,16},{10,18},{12,20},{14,22},{16,24},... | collective-permute-start | bytes 196616 | tf_op jit(solution)/shard_map/ppermute | solution.py:35
  17.7 4.1 %collective-permute-start.3 = (bf16[64,512]{1,0:T(8,128)(2,1)S(1)}, bf16[64,512]{1,0:T(8,128)(2,1)S(1)}, u32[]{:S(2)}, u32[]{:S(2)}) collective-permute-start(bf16[64,512]{1,0:T(8,128)(2,1)S(1)} %get-tuple-element.29), channel_id=1, source_target_pairs={{0,16},{2,18},{4,20},{6,22},{8,24},{10,26},{12,28},{14,30},{1,17},... | collective-permute-start | bytes 196616 | tf_op jit(solution)/shard_map/ppermute | solution.py:35
  24.3 5.0 %collective-permute-start.4 = (bf16[4,64,256]{2,1,0:T(8,128)(2,1)S(1)}, bf16[4,64,256]{2,1,0:T(8,128)(2,1)S(1)}, u32[]{:S(2)}, u32[]{:S(2)}) collective-permute-start(bf16[4,64,256]{2,1,0:T(8,128)(2,1)S(1)} %get-tuple-element.31), channel_id=1, source_target_pairs={{0,1},{1,0},{2,3},{3,2},{4,5},{5,4},{6,7},{7,6},{8,9},{9,8},{10,11... | collective-permute-start | bytes 393224 | tf_op jit(solution)/shard_map/ppermute | solution.py:378
  35.4 73.1 %all-to-all-start.1 = ((bf16[16,32,2048]{2,1,0:T(8,128)(2,1)}), bf16[16,32,2048]{2,1,0:T(8,128)(2,1)}, u32[]{:S(2)}, u32[]{:S(2)}) async-start(bf16[16,32,2048]{2,1,0:T(8,128)(2,1)} %bitcast.30), calls=%async_computation.1 | async-start | bytes 4194304 | tf_op jit(solution)/shard_map/all_to_all | solution.py:397
  42.3 61.5 %collective-permute-start.8 = (bf16[256,2048]{1,0:T(8,128)(2,1)}, bf16[256,2048]{1,0:T(8,128)(2,1)S(1)}, u32[]{:S(2)}, u32[]{:S(2)}) collective-permute-start(bf16[256,2048]{1,0:T(8,128)(2,1)} %refs_0_.1), channel_id=1, source_target_pairs={{8,16},{16,8},{9,17},{17,9},{10,18},{18,10},{11,19},{19,11},{12,20... | collective-permute-start | bytes 3145736 | tf_op jit(solution)/shard_map/ppermute | solution.py:30
  46.2 4.9 %collective-permute-start.6 = (bf16[128,2048]{1,0:T(8,128)(2,1)}, bf16[128,2048]{1,0:T(8,128)(2,1)}, u32[]{:S(2)}, u32[]{:S(2)}) collective-permute-start(bf16[128,2048]{1,0:T(8,128)(2,1)} %get-tuple-element.38), channel_id=1, source_target_pairs={{0,24},{24,0},{1,25},{25,1},{2,26},{26,2},{3,27},{27,3},{4,28},{28... | collective-permute-start | bytes 1572872 | tf_op jit(solution)/shard_map/ppermute | solution.py:30
  47.7 3.4 %collective-permute-start.7 = (bf16[128,2048]{1,0:T(8,128)(2,1)}, bf16[128,2048]{1,0:T(8,128)(2,1)}, u32[]{:S(2)}, u32[]{:S(2)}) collective-permute-start(bf16[128,2048]{1,0:T(8,128)(2,1)} %get-tuple-element.39), channel_id=1, source_target_pairs={{0,24},{24,0},{1,25},{25,1},{2,26},{26,2},{3,27},{27,3},{4,28},{28... | collective-permute-start | bytes 1572872 | tf_op jit(solution)/shard_map/ppermute | solution.py:30
  49.2 54.6 %collective-permute-start.5 = (bf16[256,512]{1,0:T(8,128)(2,1)S(1)}, bf16[256,512]{1,0:T(8,128)(2,1)}, u32[]{:S(2)}, u32[]{:S(2)}) collective-permute-start(bf16[256,512]{1,0:T(8,128)(2,1)S(1)} %shard_map.139.mapped_ref), channel_id=1, source_target_pairs={{0,24},{8,16},{16,8},{24,0},{1,25},{9,17},{17,9},{25,1},{2,26},{10... | collective-permute-start | bytes 786440 | tf_op jit(solution)/shard_map/ppermute | solution.py:30
  108.6 30.3 %all-to-all-start.4 = ((bf16[16,32,2048]{2,1,0:T(8,128)(2,1)}), bf16[16,32,2048]{2,1,0:T(8,128)(2,1)S(1)}, u32[]{:S(2)}, u32[]{:S(2)}) async-start(bf16[16,32,2048]{2,1,0:T(8,128)(2,1)} %bitcast.28), calls=%async_computation.4 | async-start | bytes 4194304 | tf_op jit(solution)/shard_map/all_to_all | solution.py:397
  138.9 21.1 %all-to-all-start.3 = ((bf16[16,32,1024]{2,1,0:T(8,128)(2,1)}), bf16[16,32,1024]{2,1,0:T(8,128)(2,1)S(1)}, u32[]{:S(2)}, u32[]{:S(2)}) async-start(bf16[16,32,1024]{2,1,0:T(8,128)(2,1)} %bitcast.32), calls=%async_computation.3 | async-start | bytes 2097152 | tf_op jit(solution)/shard_map/all_to_all | solution.py:397
  156.5 8.1 %copy-start.4 = (bf16[512,1024]{1,0:T(8,128)(2,1)S(1)}, bf16[512,1024]{1,0:T(8,128)(2,1)}, u32[]{:S(2)}) copy-start(bf16[512,1024]{1,0:T(8,128)(2,1)} %get-tuple-element.41.hidden_ref) | copy-start | bytes 3145732
  160.0 18.8 %all-to-all-start.5 = ((bf16[16,32,1024]{2,1,0:T(8,128)(2,1)}), bf16[16,32,1024]{2,1,0:T(8,128)(2,1)S(1)}, u32[]{:S(2)}, u32[]{:S(2)}) async-start(bf16[16,32,1024]{2,1,0:T(8,128)(2,1)} %bitcast.33), calls=%async_computation.5 | async-start | bytes 2097152 | tf_op jit(solution)/shard_map/all_to_all | solution.py:397
  197.1 18.2 %all-to-all-start.2 = ((bf16[16,32,1024]{2,1,0:T(8,128)(2,1)}), bf16[16,32,1024]{2,1,0:T(8,128)(2,1)}, u32[]{:S(2)}, u32[]{:S(2)}) async-start(bf16[16,32,1024]{2,1,0:T(8,128)(2,1)} %bitcast.31), calls=%async_computation.2 | async-start | bytes 2097152 | tf_op jit(solution)/shard_map/all_to_all | solution.py:397
  201.9 5.5 %copy-start.2 = (bf16[256,512]{1,0:T(8,128)(2,1)S(1)}, bf16[256,512]{1,0:T(8,128)(2,1)}, u32[]{:S(2)}) copy-start(bf16[256,512]{1,0:T(8,128)(2,1)} %get-tuple-element.25.weight_ref) | copy-start | bytes 786436
  201.9 1.0 copy-start.3
  204.1 37.6 %collective-permute-start.9 = (bf16[256,1024]{1,0:T(8,128)(2,1)}, bf16[256,1024]{1,0:T(8,128)(2,1)}, u32[]{:S(2)}, u32[]{:S(2)}) collective-permute-start(bf16[256,1024]{1,0:T(8,128)(2,1)} %shard_map.147), channel_id=1, source_target_pairs={{0,24},{8,16},{16,8},{24,0},{1,25},{9,17},{17,9},{25,1},{2,26},{10... | collective-permute-start | bytes 1572872 | tf_op jit(solution)/shard_map/ppermute | solution.py:30
  205.9 46.2 %collective-permute-start.10 = (bf16[256,1024]{1,0:T(8,128)(2,1)}, bf16[256,1024]{1,0:T(8,128)(2,1)}, u32[]{:S(2)}, u32[]{:S(2)}) collective-permute-start(bf16[256,1024]{1,0:T(8,128)(2,1)} %shard_map.149), channel_id=1, source_target_pairs={{0,24},{8,16},{16,8},{24,0},{1,25},{9,17},{17,9},{25,1},{2,26},{10... | collective-permute-start | bytes 1572872 | tf_op jit(solution)/shard_map/ppermute | solution.py:30
  207.4 44.7 %copy-start.1 = (bf16[256,2048]{1,0:T(8,128)(2,1)S(1)}, bf16[256,2048]{1,0:T(8,128)(2,1)}, u32[]{:S(2)}) copy-start(bf16[256,2048]{1,0:T(8,128)(2,1)} %get-tuple-element.42.stream_ref) | copy-start | bytes 3145732

commit v4 on v3

--- a/solution.py
+++ b/solution.py
@@ -432,12 +432,17 @@
             own_weight, own_back,
             vmem=big,
         )
-    (out,) = call(
+    step = rows // 4
+    inputs = [*own_sums, *others, stream, in_hbm(out_gain.reshape(1, -1))]
+    specs = [pl.BlockSpec((step, v.shape[1]), lambda i: (i, 0)) for v in inputs[:-1]]
+    out = pl.pallas_call(
         last_kernel,
-        [((rows, width), BF16)],
-        *own_sums, *others, stream, in_hbm(out_gain.reshape(1, -1)),
-        vmem=big,
-    )
+        grid=(rows // step,),
+        out_shape=jax.ShapeDtypeStruct((rows, width), BF16),
+        in_specs=specs + [pl.BlockSpec((1, width), lambda i: (0, 0))],
+        out_specs=pl.BlockSpec((step, width), lambda i: (i, 0)),
+        compiler_params=pltpu.CompilerParams(vmem_limit_bytes=16 * 2**20),
+    )(*inputs)
     return out
 
 

time: 256 us -> 257 us (level)
    pallas_call x0 -> x1, Pallas kernels: none -> 3.78 us  [local(): pl.pallas_call(last_kernel, grid=(rows // step,), out_shape=jax.ShapeDtyp...]
    pallas_call x12 -> x11, Pallas kernels: 27.3 us -> 24.2 us  [call(): pl.pallas_call(kernel, out_shape=shapes, in_specs=specs, out_specs=[VM] *...]
where the time goes in v4:
time: 257 us; the launch traced here: 256 us
  waiting for transfers between devices  124 us (48%)
  starting transfers between devices  56.5 us (22%)
  Pallas kernels  55.4 us (22%)
  blocking collectives  18.3 us (7%)
    ppermute x6, waiting for transfers between devices, to_twin(): return lax.ppermute(x, ('zh', 'zl'), [(i, last - i) for i in used])  87.8 us
    all_to_all x5, waiting for transfers between devices, there(): return lax.all_to_all(x, HALF, 0, 0, tiled=True).reshape(-1, columns)  33.1 us
    all_to_all x5, starting transfers between devices, there(): return lax.all_to_all(x, HALF, 0, 0, tiled=True).reshape(-1, columns)  28.8 us
    pallas_call x11, Pallas kernels, call(): pl.pallas_call(kernel, out_shape=shapes, in_specs=specs, out_specs=[VM] *...  24.2 us
    pallas_call x2, Pallas kernels, expert_rows(): pl.pallas_call(functools.partial(expert_kernel, tiles), grid=(tiles + par...  23.6 us
    all_to_all x1, blocking collectives, there(): return lax.all_to_all(x, HALF, 0, 0, tiled=True).reshape(-1, columns)  18.3 us
    ppermute x4, starting transfers between devices, passed_along(): return lax.ppermute(x, SP, [(i, i + by) for i in range(devices - by)])  10.9 us
    ppermute x6, starting transfers between devices, to_twin(): return lax.ppermute(x, ('zh', 'zl'), [(i, last - i) for i in used])  8.9 us
  transfers between devices with their start and end apart: 17, of which 10 were waited for; matrix products, arithmetic and copies ran while one was open for 0% of the time, Pallas kernels for 16%

profile of v4, /device:TPU:8, one launch (start us, length us, event | category | flops | bytes accessed | tf_op | source)
XLA Modules:
  0.0 255.9 jit_solution(15851194962660614906)
XLA Ops:
  0.0 0.0 copy-start
  0.0 2.6 %shard_map.136 = (f32[16,16,128]{2,1,0:T(8,128)}, bf16[64,512]{1,0:T(8,128)(2,1)S(1)}, bf16[64,512]{1,0:T(8,128)(2,1)S(1)}, bf16[64,512]{1,0:T(8,128)(2,1)S(1)},...) custom-call(bf16[4,64,512]{2,1,0:T(8,128)(2,1)} %x_ref.3, s32[1,512]{1,0:T(1,128)} %bitcast.39, ...), custom_call_target="tpu_custom_call" | custom-call | bytes 2758656 | tf_op jit(solution)/shard_map/pallas_call | solution.py:67
  2.6 6.3 %all-to-all-start = ((f32[16,16,128]{2,1,0:T(8,128)}), f32[16,16,128]{2,1,0:T(8,128)S(1)}, u32[]{:S(2)}, u32[]{:S(2)}) async-start(f32[16,16,128]{2,1,0:T(8,128)} %get-tuple-element.24), calls=%async_computation | async-start | bytes 262144 | tf_op jit(solution)/shard_map/all_to_all | solution.py:359
  8.9 2.0 collective-permute-start
  11.0 3.4 %collective-permute-start.1 = (bf16[64,512]{1,0:T(8,128)(2,1)S(1)}, bf16[64,512]{1,0:T(8,128)(2,1)S(1)}, u32[]{:S(2)}, u32[]{:S(2)}) collective-permute-start(bf16[64,512]{1,0:T(8,128)(2,1)S(1)} %get-tuple-element.27), channel_id=1, source_target_pairs={{0,4},{2,6},{4,8},{6,10},{8,12},{10,14},{12,16},{14,18},{16,20},{1... | collective-permute-start | bytes 196616 | tf_op jit(solution)/shard_map/ppermute | solution.py:35
  14.3 3.4 %collective-permute-start.2 = (bf16[64,512]{1,0:T(8,128)(2,1)S(1)}, bf16[64,512]{1,0:T(8,128)(2,1)S(1)}, u32[]{:S(2)}, u32[]{:S(2)}) collective-permute-start(bf16[64,512]{1,0:T(8,128)(2,1)S(1)} %get-tuple-element.28), channel_id=1, source_target_pairs={{0,8},{2,10},{4,12},{6,14},{8,16},{10,18},{12,20},{14,22},{16,24},... | collective-permute-start | bytes 196616 | tf_op jit(solution)/shard_map/ppermute | solution.py:35
  17.7 2.2 collective-permute-start.3
  19.9 0.1 stack.34.where_ref
  20.0 0.0 collective-permute-done.refs_0_
  20.0 0.0 collective-permute-done.1.refs_1_
  20.0 1.0 collective-permute-done.2.refs_2_
  21.0 0.8 collective-permute-done.3.refs_3_
  21.8 0.0 all-to-all-done.news_ref
  21.8 2.5 shard_map.138
  24.3 1.6 collective-permute-start.4
  25.9 1.8 shard_map.137
  27.7 1.7 collective-permute-done.4.refs_1_
  29.3 1.3 shard_map.139.mapped_ref
  30.6 0.0 copy-done
  30.6 4.8 %shard_map.140 = (bf16[512,2048]{1,0:T(8,128)(2,1)}, bf16[256,2048]{1,0:T(8,128)(2,1)}) custom-call(s32[5]{0:T(128)S(1)} %stack.34.where_ref, bf16[256,512]{1,0:T(8,128)(2,1)S(1)} %shard_map.139.mapped_ref, bf16[512,2048]{1,0:T(8,128)(2,1)S(1)} %copy-done, f32[1,2048]{1,0:T(1,128)} %bitcast.34, f32[1,2048]{1,0:T(1,128)} %bitcast.36, ...), custom_call_target="tpu_custom_call" | custom-call | bytes 6832148 | tf_op jit(solution)/shard_map/pallas_call | solution.py:67
  35.4 6.9 %all-to-all-start.1 = ((bf16[16,32,2048]{2,1,0:T(8,128)(2,1)}), bf16[16,32,2048]{2,1,0:T(8,128)(2,1)}, u32[]{:S(2)}, u32[]{:S(2)}) async-start(bf16[16,32,2048]{2,1,0:T(8,128)(2,1)} %bitcast.30), calls=%async_computation.1 | async-start | bytes 4194304 | tf_op jit(solution)/shard_map/all_to_all | solution.py:397
  42.3 3.9 %collective-permute-start.8 = (bf16[256,2048]{1,0:T(8,128)(2,1)}, bf16[256,2048]{1,0:T(8,128)(2,1)S(1)}, u32[]{:S(2)}, u32[]{:S(2)}) collective-permute-start(bf16[256,2048]{1,0:T(8,128)(2,1)} %refs_0_.1), channel_id=1, source_target_pairs={{8,16},{16,8},{9,17},{17,9},{10,18},{18,10},{11,19},{19,11},{12,20... | collective-permute-start | bytes 3145736 | tf_op jit(solution)/shard_map/ppermute | solution.py:30
  46.2 1.5 collective-permute-start.6
  47.7 1.4 collective-permute-start.7
  49.2 0.0 collective-permute-start.5
  49.2 0.1 stack.36.where_ref
  49.3 1.9 shard_map.144
  51.1 0.0 collective-permute-done.6.refs_0_
  51.1 0.0 collective-permute-done.7.refs_1_
  51.1 52.7 %collective-permute-done.5.mapped_ref = bf16[256,512]{1,0:T(8,128)(2,1)} collective-permute-done((bf16[256,512]{1,0:T(8,128)(2,1)S(1)}, bf16[256,512]{1,0:T(8,128)(2,1)}, u32[]{:S(2)}, u32[]{:S(2)}) %collective-permute-start.5) | collective-permute-done | bytes 262176 | tf_op jit(solution)/shard_map/ppermute | solution.py:30
  103.8 0.0 collective-permute-done.8.refs_2_
  103.8 4.8 %shard_map.145 = bf16[512,2048]{1,0:T(8,128)(2,1)} custom-call(s32[5]{0:T(128)S(1)} %stack.36.where_ref, bf16[256,512]{1,0:T(8,128)(2,1)} %collective-permute-done.5.mapped_ref, bf16[512,2048]{1,0:T(8,128)(2,1)S(1)} %copy-done, f32[1,2048]{1,0:T(1,128)} %bitcast.35, f32[1,2048]{1,0:T(1,128)} %bitcast.37, bf16[512,256]{1,0:T(8,128)(2,1)S(1)} %get-tuple-element.37.pick_ref, ...), custom_call_target="tpu_custom_call" | custom-call | bytes 6832148 | tf_op jit(solution)/shard_map/pallas_call | solution.py:67
  108.6 0.0 all-to-all-done.1
  108.6 5.3 %all-to-all-start.4 = ((bf16[16,32,2048]{2,1,0:T(8,128)(2,1)}), bf16[16,32,2048]{2,1,0:T(8,128)(2,1)S(1)}, u32[]{:S(2)}, u32[]{:S(2)}) async-start(bf16[16,32,2048]{2,1,0:T(8,128)(2,1)} %bitcast.28), calls=%async_computation.4 | async-start | bytes 4194304 | tf_op jit(solution)/shard_map/all_to_all | solution.py:397
  113.9 13.3 %shard_map.141 = (bf16[512,1024]{1,0:T(8,128)(2,1)}, bf16[512,1024]{1,0:T(8,128)(2,1)}, bf16[512,1024]{1,0:T(8,128)(2,1)}) custom-call(bf16[512,2048]{1,0:T(8,128)(2,1)} %bitcast.11.x_ref, bf16[1,2048,1024]{2,1,0:T(8,128)(2,1)} %gate_ref.3, bf16[1,2048,1024]{2,1,0:T(8,128)(2,1)} %up_ref.3, bf16[1,1024,2048]{2,1,0:T(8,128)(2,1)} %down_ref.5), custom_call_target="tpu_custom_call" | custom-call | flops 6442450944 | bytes 16777216 | tf_op jit(solution)/shard_map/pallas_call | solution.py:259
  127.2 11.6 %all-to-all-done.4 = bf16[16,32,2048]{2,1,0:T(8,128)(2,1)S(1)} async-done(((bf16[16,32,2048]{2,1,0:T(8,128)(2,1)}), bf16[16,32,2048]{2,1,0:T(8,128)(2,1)S(1)}, u32[]{:S(2)}, u32[]{:S(2)}) %all-to-all-start.4) | async-done | bytes 2097184 | tf_op jit(solution)/shard_map/all_to_all | solution.py:397
  138.9 7.3 %all-to-all-start.3 = ((bf16[16,32,1024]{2,1,0:T(8,128)(2,1)}), bf16[16,32,1024]{2,1,0:T(8,128)(2,1)S(1)}, u32[]{:S(2)}, u32[]{:S(2)}) async-start(bf16[16,32,1024]{2,1,0:T(8,128)(2,1)} %bitcast.32), calls=%async_computation.3 | async-start | bytes 2097152 | tf_op jit(solution)/shard_map/all_to_all | solution.py:397
  146.2 10.3 %shard_map.146 = (bf16[512,1024]{1,0:T(8,128)(2,1)}, bf16[512,1024]{1,0:T(8,128)(2,1)}) custom-call(bf16[512,2048]{1,0:T(8,128)(2,1)S(1)} %bitcast.27, bf16[1,2048,1024]{2,1,0:T(8,128)(2,1)} %gate_ref.3, bf16[1,2048,1024]{2,1,0:T(8,128)(2,1)} %up_ref.3, bf16[1,1024,2048]{2,1,0:T(8,128)(2,1)} %down_ref.5), custom_call_target="tpu_custom_call" | custom-call | flops 5368709120 | bytes 14680064 | tf_op jit(solution)/shard_map/pallas_call | solution.py:259
  156.5 0.0 copy-start.4
  156.5 3.5 %all-to-all-done.3 = bf16[16,32,1024]{2,1,0:T(8,128)(2,1)S(1)} async-done(((bf16[16,32,1024]{2,1,0:T(8,128)(2,1)}), bf16[16,32,1024]{2,1,0:T(8,128)(2,1)S(1)}, u32[]{:S(2)}, u32[]{:S(2)}) %all-to-all-start.3) | async-done | bytes 1048608 | tf_op jit(solution)/shard_map/all_to_all | solution.py:397
  160.0 4.6 %all-to-all-start.5 = ((bf16[16,32,1024]{2,1,0:T(8,128)(2,1)}), bf16[16,32,1024]{2,1,0:T(8,128)(2,1)S(1)}, u32[]{:S(2)}, u32[]{:S(2)}) async-start(bf16[16,32,1024]{2,1,0:T(8,128)(2,1)} %bitcast.33), calls=%async_computation.5 | async-start | bytes 2097152 | tf_op jit(solution)/shard_map/all_to_all | solution.py:397
  164.6 0.0 copy-done.4
  164.6 3.8 %shard_map.148 = bf16[512,1024]{1,0:T(8,128)(2,1)} custom-call(bf16[512,1024]{1,0:T(8,128)(2,1)S(1)} %copy-done.4, bf16[1,1024,2048]{2,1,0:T(8,128)(2,1)} %down_ref.5), custom_call_target="tpu_custom_call" | custom-call | flops 1073741824 | bytes 4194304 | tf_op jit(solution)/shard_map/pallas_call | solution.py:290
  168.4 10.4 %all-to-all-done.5 = bf16[16,32,1024]{2,1,0:T(8,128)(2,1)S(1)} async-done(((bf16[16,32,1024]{2,1,0:T(8,128)(2,1)}), bf16[16,32,1024]{2,1,0:T(8,128)(2,1)S(1)}, u32[]{:S(2)}, u32[]{:S(2)}) %all-to-all-start.5) | async-done | bytes 1048608 | tf_op jit(solution)/shard_map/all_to_all | solution.py:397
  178.8 18.3 %all_to_all.35 = bf16[16,32,1024]{2,1,0:T(8,128)(2,1)S(1)} all-to-all(bf16[16,32,1024]{2,1,0:T(8,128)(2,1)} %bitcast.29), channel_id=1, replica_groups=mesh['zh'=2,'zl'=2,'yc'=4,'tp'=2] {'zl','yc','tp'}, dimensions={0} | all-to-all | bytes 2097152 | tf_op jit(solution)/shard_map/all_to_all | solution.py:397
  197.1 4.8 %all-to-all-start.2 = ((bf16[16,32,1024]{2,1,0:T(8,128)(2,1)}), bf16[16,32,1024]{2,1,0:T(8,128)(2,1)}, u32[]{:S(2)}, u32[]{:S(2)}) async-start(bf16[16,32,1024]{2,1,0:T(8,128)(2,1)} %bitcast.31), calls=%async_computation.2 | async-start | bytes 2097152 | tf_op jit(solution)/shard_map/all_to_all | solution.py:397
  201.9 0.0 copy-start.2
  201.9 0.0 copy-start.3
  201.9 1.0 copy-done.3
  202.9 1.2 shard_map.147
  204.1 0.5 collective-permute-start.9
  204.6 1.2 shard_map.149
  205.9 1.5 collective-permute-start.10
  207.4 0.0 copy-done.2
  207.4 0.0 copy-start.1
  207.4 0.4 shard_map.143.own_1
  207.8 7.5 %all-to-all-done.2 = bf16[16,32,1024]{2,1,0:T(8,128)(2,1)} async-done(((bf16[16,32,1024]{2,1,0:T(8,128)(2,1)}), bf16[16,32,1024]{2,1,0:T(8,128)(2,1)}, u32[]{:S(2)}, u32[]{:S(2)}) %all-to-all-start.2) | async-done | bytes 1048608 | tf_op jit(solution)/shard_map/all_to_all | solution.py:397
  215.3 1.7 shard_map.142.own_0
  217.0 24.7 %collective-permute-done.9.other_0 = bf16[256,1024]{1,0:T(8,128)(2,1)} collective-permute-done((bf16[256,1024]{1,0:T(8,128)(2,1)}, bf16[256,1024]{1,0:T(8,128)(2,1)}, u32[]{:S(2)}, u32[]{:S(2)}) %collective-permute-start.9) | collective-permute-done | bytes 524320 | tf_op jit(solution)/shard_map/ppermute | solution.py:30
  241.7 10.4 %collective-permute-done.10.other_1 = bf16[256,1024]{1,0:T(8,128)(2,1)} collective-permute-done((bf16[256,1024]{1,0:T(8,128)(2,1)}, bf16[256,1024]{1,0:T(8,128)(2,1)}, u32[]{:S(2)}, u32[]{:S(2)}) %collective-permute-start.10) | collective-permute-done | bytes 524320 | tf_op jit(solution)/shard_map/ppermute | solution.py:30
  252.1 0.0 copy-done.1
  252.1 3.8 %shard_map.150 = bf16[256,2048]{1,0:T(8,128)(2,1)} custom-call(f32[256,1024]{1,0:T(8,128)S(1)} %shard_map.142.own_0, f32[256,1024]{1,0:T(8,128)S(1)} %shard_map.143.own_1, bf16[256,1024]{1,0:T(8,128)(2,1)} %collective-permute-done.9.other_0, bf16[256,1024]{1,0:T(8,128)(2,1)} %collective-permute-done.10.other_1, bf16[256,2048]{1,0:T(8,128)(2,1)S(1)} %copy-done.1, ...), custom_call_target="tpu_custom_call" | custom-call | tf_op jit(solution)/shard_map/pallas_call | solution.py:438
Async XLA Ops:
  0.0 30.6 %copy-start = (bf16[512,2048]{1,0:T(8,128)(2,1)S(1)}, bf16[512,2048]{1,0:T(8,128)(2,1)}, u32[]{:S(2)}) copy-start(bf16[512,2048]{1,0:T(8,128)(2,1)} %w_ref.3) | copy-start | bytes 6291460
  2.6 19.2 %all-to-all-start = ((f32[16,16,128]{2,1,0:T(8,128)}), f32[16,16,128]{2,1,0:T(8,128)S(1)}, u32[]{:S(2)}, u32[]{:S(2)}) async-start(f32[16,16,128]{2,1,0:T(8,128)} %get-tuple-element.24), calls=%async_computation | async-start | bytes 262144 | tf_op jit(solution)/shard_map/all_to_all | solution.py:359
  8.9 11.1 %collective-permute-start = (bf16[64,512]{1,0:T(8,128)(2,1)S(1)}, bf16[64,512]{1,0:T(8,128)(2,1)S(1)}, u32[]{:S(2)}, u32[]{:S(2)}) collective-permute-start(bf16[64,512]{1,0:T(8,128)(2,1)S(1)} %get-tuple-element.26), channel_id=1, source_target_pairs={{0,2},{2,4},{4,6},{6,8},{8,10},{10,12},{12,14},{14,16},{16,18},{18... | collective-permute-start | bytes 196616 | tf_op jit(solution)/shard_map/ppermute | solution.py:35
  11.0 9.1 %collective-permute-start.1 = (bf16[64,512]{1,0:T(8,128)(2,1)S(1)}, bf16[64,512]{1,0:T(8,128)(2,1)S(1)}, u32[]{:S(2)}, u32[]{:S(2)}) collective-permute-start(bf16[64,512]{1,0:T(8,128)(2,1)S(1)} %get-tuple-element.27), channel_id=1, source_target_pairs={{0,4},{2,6},{4,8},{6,10},{8,12},{10,14},{12,16},{14,18},{16,20},{1... | collective-permute-start | bytes 196616 | tf_op jit(solution)/shard_map/ppermute | solution.py:35
  14.3 6.6 %collective-permute-start.2 = (bf16[64,512]{1,0:T(8,128)(2,1)S(1)}, bf16[64,512]{1,0:T(8,128)(2,1)S(1)}, u32[]{:S(2)}, u32[]{:S(2)}) collective-permute-start(bf16[64,512]{1,0:T(8,128)(2,1)S(1)} %get-tuple-element.28), channel_id=1, source_target_pairs={{0,8},{2,10},{4,12},{6,14},{8,16},{10,18},{12,20},{14,22},{16,24},... | collective-permute-start | bytes 196616 | tf_op jit(solution)/shard_map/ppermute | solution.py:35
  17.7 4.1 %collective-permute-start.3 = (bf16[64,512]{1,0:T(8,128)(2,1)S(1)}, bf16[64,512]{1,0:T(8,128)(2,1)S(1)}, u32[]{:S(2)}, u32[]{:S(2)}) collective-permute-start(bf16[64,512]{1,0:T(8,128)(2,1)S(1)} %get-tuple-element.29), channel_id=1, source_target_pairs={{0,16},{2,18},{4,20},{6,22},{8,24},{10,26},{12,28},{14,30},{1,17},... | collective-permute-start | bytes 196616 | tf_op jit(solution)/shard_map/ppermute | solution.py:35
  24.3 5.0 %collective-permute-start.4 = (bf16[4,64,256]{2,1,0:T(8,128)(2,1)S(1)}, bf16[4,64,256]{2,1,0:T(8,128)(2,1)S(1)}, u32[]{:S(2)}, u32[]{:S(2)}) collective-permute-start(bf16[4,64,256]{2,1,0:T(8,128)(2,1)S(1)} %get-tuple-element.31), channel_id=1, source_target_pairs={{0,1},{1,0},{2,3},{3,2},{4,5},{5,4},{6,7},{7,6},{8,9},{9,8},{10,11... | collective-permute-start | bytes 393224 | tf_op jit(solution)/shard_map/ppermute | solution.py:378
  35.4 73.1 %all-to-all-start.1 = ((bf16[16,32,2048]{2,1,0:T(8,128)(2,1)}), bf16[16,32,2048]{2,1,0:T(8,128)(2,1)}, u32[]{:S(2)}, u32[]{:S(2)}) async-start(bf16[16,32,2048]{2,1,0:T(8,128)(2,1)} %bitcast.30), calls=%async_computation.1 | async-start | bytes 4194304 | tf_op jit(solution)/shard_map/all_to_all | solution.py:397
  42.3 61.5 %collective-permute-start.8 = (bf16[256,2048]{1,0:T(8,128)(2,1)}, bf16[256,2048]{1,0:T(8,128)(2,1)S(1)}, u32[]{:S(2)}, u32[]{:S(2)}) collective-permute-start(bf16[256,2048]{1,0:T(8,128)(2,1)} %refs_0_.1), channel_id=1, source_target_pairs={{8,16},{16,8},{9,17},{17,9},{10,18},{18,10},{11,19},{19,11},{12,20... | collective-permute-start | bytes 3145736 | tf_op jit(solution)/shard_map/ppermute | solution.py:30
  46.2 4.9 %collective-permute-start.6 = (bf16[128,2048]{1,0:T(8,128)(2,1)}, bf16[128,2048]{1,0:T(8,128)(2,1)}, u32[]{:S(2)}, u32[]{:S(2)}) collective-permute-start(bf16[128,2048]{1,0:T(8,128)(2,1)} %get-tuple-element.38), channel_id=1, source_target_pairs={{0,24},{24,0},{1,25},{25,1},{2,26},{26,2},{3,27},{27,3},{4,28},{28... | collective-permute-start | bytes 1572872 | tf_op jit(solution)/shard_map/ppermute | solution.py:30
  47.7 3.4 %collective-permute-start.7 = (bf16[128,2048]{1,0:T(8,128)(2,1)}, bf16[128,2048]{1,0:T(8,128)(2,1)}, u32[]{:S(2)}, u32[]{:S(2)}) collective-permute-start(bf16[128,2048]{1,0:T(8,128)(2,1)} %get-tuple-element.39), channel_id=1, source_target_pairs={{0,24},{24,0},{1,25},{25,1},{2,26},{26,2},{3,27},{27,3},{4,28},{28... | collective-permute-start | bytes 1572872 | tf_op jit(solution)/shard_map/ppermute | solution.py:30
  49.2 54.6 %collective-permute-start.5 = (bf16[256,512]{1,0:T(8,128)(2,1)S(1)}, bf16[256,512]{1,0:T(8,128)(2,1)}, u32[]{:S(2)}, u32[]{:S(2)}) collective-permute-start(bf16[256,512]{1,0:T(8,128)(2,1)S(1)} %shard_map.139.mapped_ref), channel_id=1, source_target_pairs={{0,24},{8,16},{16,8},{24,0},{1,25},{9,17},{17,9},{25,1},{2,26},{10... | collective-permute-start | bytes 786440 | tf_op jit(solution)/shard_map/ppermute | solution.py:30
  108.6 30.3 %all-to-all-start.4 = ((bf16[16,32,2048]{2,1,0:T(8,128)(2,1)}), bf16[16,32,2048]{2,1,0:T(8,128)(2,1)S(1)}, u32[]{:S(2)}, u32[]{:S(2)}) async-start(bf16[16,32,2048]{2,1,0:T(8,128)(2,1)} %bitcast.28), calls=%async_computation.4 | async-start | bytes 4194304 | tf_op jit(solution)/shard_map/all_to_all | solution.py:397
  138.9 21.1 %all-to-all-start.3 = ((bf16[16,32,1024]{2,1,0:T(8,128)(2,1)}), bf16[16,32,1024]{2,1,0:T(8,128)(2,1)S(1)}, u32[]{:S(2)}, u32[]{:S(2)}) async-start(bf16[16,32,1024]{2,1,0:T(8,128)(2,1)} %bitcast.32), calls=%async_computation.3 | async-start | bytes 2097152 | tf_op jit(solution)/shard_map/all_to_all | solution.py:397
  156.5 8.1 %copy-start.4 = (bf16[512,1024]{1,0:T(8,128)(2,1)S(1)}, bf16[512,1024]{1,0:T(8,128)(2,1)}, u32[]{:S(2)}) copy-start(bf16[512,1024]{1,0:T(8,128)(2,1)} %get-tuple-element.41.hidden_ref) | copy-start | bytes 3145732
  160.0 18.8 %all-to-all-start.5 = ((bf16[16,32,1024]{2,1,0:T(8,128)(2,1)}), bf16[16,32,1024]{2,1,0:T(8,128)(2,1)S(1)}, u32[]{:S(2)}, u32[]{:S(2)}) async-start(bf16[16,32,1024]{2,1,0:T(8,128)(2,1)} %bitcast.33), calls=%async_computation.5 | async-start | bytes 2097152 | tf_op jit(solution)/shard_map/all_to_all | solution.py:397
  197.1 18.2 %all-to-all-start.2 = ((bf16[16,32,1024]{2,1,0:T(8,128)(2,1)}), bf16[16,32,1024]{2,1,0:T(8,128)(2,1)}, u32[]{:S(2)}, u32[]{:S(2)}) async-start(bf16[16,32,1024]{2,1,0:T(8,128)(2,1)} %bitcast.31), calls=%async_computation.2 | async-start | bytes 2097152 | tf_op jit(solution)/shard_map/all_to_all | solution.py:397
  201.9 5.5 %copy-start.2 = (bf16[256,512]{1,0:T(8,128)(2,1)S(1)}, bf16[256,512]{1,0:T(8,128)(2,1)}, u32[]{:S(2)}) copy-start(bf16[256,512]{1,0:T(8,128)(2,1)} %get-tuple-element.25.weight_ref) | copy-start | bytes 786436
  201.9 1.0 copy-start.3
  204.1 37.6 %collective-permute-start.9 = (bf16[256,1024]{1,0:T(8,128)(2,1)}, bf16[256,1024]{1,0:T(8,128)(2,1)}, u32[]{:S(2)}, u32[]{:S(2)}) collective-permute-start(bf16[256,1024]{1,0:T(8,128)(2,1)} %shard_map.147), channel_id=1, source_target_pairs={{0,24},{8,16},{16,8},{24,0},{1,25},{9,17},{17,9},{25,1},{2,26},{10... | collective-permute-start | bytes 1572872 | tf_op jit(solution)/shard_map/ppermute | solution.py:30
  205.9 46.2 %collective-permute-start.10 = (bf16[256,1024]{1,0:T(8,128)(2,1)}, bf16[256,1024]{1,0:T(8,128)(2,1)}, u32[]{:S(2)}, u32[]{:S(2)}) collective-permute-start(bf16[256,1024]{1,0:T(8,128)(2,1)} %shard_map.149), channel_id=1, source_target_pairs={{0,24},{8,16},{16,8},{24,0},{1,25},{9,17},{17,9},{25,1},{2,26},{10... | collective-permute-start | bytes 1572872 | tf_op jit(solution)/shard_map/ppermute | solution.py:30
  207.4 44.7 %copy-start.1 = (bf16[256,2048]{1,0:T(8,128)(2,1)S(1)}, bf16[256,2048]{1,0:T(8,128)(2,1)}, u32[]{:S(2)}) copy-start(bf16[256,2048]{1,0:T(8,128)(2,1)} %get-tuple-element.42.stream_ref) | copy-start | bytes 3145732
